TPU v7x, 32 devices: a whole 2x2x4 slice. The times are simulated.
32 devices in a mesh: ep: 8 (over z, core), tp: 4 (over y, x).
Axes of the slice: x: 2, y: 2, z: 4, core: 2. Of those that a mesh axis runs over, the one named last changes fastest.
Arguments:
- receptance: bfloat16 [2048, 2048], P('ep', 'tp'), may hold values from -6 to 6
- key_in: bfloat16 [2048, 2048], P('ep', 'tp'), may hold values from -6 to 6
- value_in: bfloat16 [2048, 2048], P('ep', 'tp'), may hold values from -6 to 6
- decay_in: bfloat16 [2048, 2048], P('ep', 'tp'), may hold values from -16 to 2
- rate_in: bfloat16 [2048, 2048], P('ep', 'tp'), may hold values from -12 to 4
- norm_gain: float32 [2048], P('tp'), may hold values from 0.1 to 1.9
- out_weight: bfloat16 [2048, 4096], P('tp'), may hold values from -0.125 to 0.125
- moe_in: bfloat16 [1024, 4096], P('ep'), may hold values from -6 to 6
- ffn_gain: float32 [4096], replicated, may hold values from 0.1 to 1.9
- routes: int32 [1024, 4], P('ep'), may hold values from 0 to 7, all different within a row; in each aligned block of 128 rows (0 to 127, 128 to 255, ...) at most 80 rows name the same one
- route_weights: float32 [1024, 4], P('ep'), may hold values from 0.2 to 1
- gate_weight: bfloat16 [8, 4096, 1024], P('ep', None, 'tp'), may hold values from -0.09375 to 0.09375
- up_weight: bfloat16 [8, 4096, 1024], P('ep', None, 'tp'), may hold values from -0.09375 to 0.09375
- down_weight: bfloat16 [8, 1024, 4096], P('ep', None, 'tp'), may hold values from -0.1875 to 0.1875
Outputs:
- mixer_out: bfloat16 [2048, 4096], P(('ep', 'tp'))
- moe_out: bfloat16 [1024, 4096], P('ep', 'tp')
Inputs may be any that keep to these rules, and one draw needn't show every extreme that they name: `routes`: A row names 4 different experts. Among the 128 rows that one index of ep holds, no expert is named by more than 80 rows, and in every draw some expert is named by exactly 80 of them.
All inputs are finite; a program needn't handle non-finite values.
Results may differ from a plain program's by a relative error of at most 0.025.
Values may be sent and summed in bfloat16 or wider, within the bound.
A program may use at most 64 MiB of HBM per device.

v0:
```python
import functools

import jax
import jax.numpy as jnp
from jax import lax
from jax.experimental import pallas as pl
from jax.experimental.pallas import tpu as pltpu
from jax.sharding import PartitionSpec as P

HD = 64
BLOCK = 64
F32 = jnp.float32
BF16 = jnp.bfloat16
MESH = pl.DeviceIdType.MESH


def dot(a, b):
    return jnp.dot(a.astype(BF16), b.astype(BF16), preferred_element_type=F32)


def dot_rows(a, b):
    return lax.dot_general(
        a.astype(BF16), b.astype(BF16), (((1,), (1,)), ((), ())), preferred_element_type=F32
    )


def dot_cols(a, b):
    return lax.dot_general(
        a.astype(BF16), b.astype(BF16), (((0,), (0,)), ((), ())), preferred_element_type=F32
    )


def dot_exact(a, b):
    return jnp.dot(a, b, precision=lax.Precision.HIGHEST, preferred_element_type=F32)


def lane_head(rows, width):
    return lax.broadcasted_iota(jnp.int32, (rows, width), 1) // HD


def spread(packed):
    rows, width = packed.shape
    packed = packed.astype(BF16)
    head = lane_head(rows, width)
    return jnp.concatenate(
        [jnp.where(head == i, packed, jnp.zeros_like(packed)) for i in range(width // HD)], axis=0
    )


def fold(square):
    width = square.shape[1]
    head = lane_head(HD, width)
    out = jnp.zeros((HD, width), F32)
    for i in range(width // HD):
        out = jnp.where(head == i, square[i * HD : (i + 1) * HD], out)
    return out


def head_ones(width):
    row = lax.broadcasted_iota(jnp.int32, (width, width), 0) // HD
    return (row == lane_head(width, width)).astype(F32)


def group_width(columns):
    return HD * max(g for g in (4, 2, 1) if columns % (g * HD) == 0)


def tables_kernel(r_ref, k_ref, v_ref, d_ref, a_ref, read_ref, local_ref, total_ref, carry):
    columns = r_ref.shape[1]
    width = group_width(columns)
    row = lax.broadcasted_iota(jnp.int32, (BLOCK, width), 0)
    lane = lax.broadcasted_iota(jnp.int32, (BLOCK, width), 1) % HD
    strict = lane < row
    closed = lane <= row
    eye = (lane == row).astype(F32)
    tril = (
        lax.broadcasted_iota(jnp.int32, (BLOCK, BLOCK), 1)
        <= lax.broadcasted_iota(jnp.int32, (BLOCK, BLOCK), 0)
    ).astype(F32)
    ones = head_ones(width)

    @pl.when(pl.program_id(0) == 0)
    def _():
        for group in range(columns // width):
            carry[0, group] = eye
            carry[1, group] = jnp.zeros_like(eye)

    for group in range(columns // width):
        at = pl.ds(group * width, width)
        readout = r_ref[:, at].astype(F32)
        key = k_ref[:, at].astype(F32)
        value = v_ref[:, at]
        log_decay = jax.nn.sigmoid(d_ref[:, at].astype(F32)) * -0.6065306597126334
        rate = jax.nn.sigmoid(a_ref[:, at].astype(F32))
        unit = key * lax.rsqrt(dot_exact(key * key, ones) + 1.0)
        inclusive = dot_exact(tril, log_decay)
        total = inclusive[BLOCK - 1 :]
        probe = -unit * jnp.exp(inclusive - log_decay)
        removal = unit * rate
        written = key * rate
        back = jnp.exp(-inclusive)
        tail = jnp.exp(total - inclusive)
        readout = readout * jnp.exp(inclusive)
        left = jnp.concatenate([probe, readout], axis=0)
        on_removal = dot_rows(left, spread(removal * back))
        on_write = dot_rows(left, spread(written * back))
        lower = jnp.where(strict, on_removal[:BLOCK], 0.0)
        reach = jnp.where(closed, on_removal[BLOCK:], 0.0)
        lower_write = jnp.where(strict, on_write[:BLOCK], 0.0)
        reach_write = jnp.where(closed, on_write[BLOCK:], 0.0)
        value_wide = spread(value)
        on_value = dot(jnp.concatenate([lower_write, reach_write], axis=0), value_wide)
        inverse = eye + lower
        power = dot(lower, spread(lower))
        for doubling in range(BLOCK.bit_length() - 2):
            wide = spread(power)
            if doubling < BLOCK.bit_length() - 3:
                both = dot(jnp.concatenate([inverse, power], axis=0), wide)
                inverse = inverse + both[:BLOCK]
                power = both[BLOCK:]
            else:
                inverse = inverse + dot(inverse, wide)
        solved_probe = dot(inverse, spread(probe))
        solved_values = dot(inverse, spread(on_value[:BLOCK]))
        transition = eye * jnp.exp(total) + fold(dot_cols(removal * tail, solved_probe))
        increment = fold(
            dot_cols(
                jnp.concatenate([removal * tail, written * tail], axis=0),
                jnp.concatenate([solved_values.astype(BF16), value], axis=0),
            )
        )
        read_state = readout + dot(reach, spread(solved_probe))
        local_out = dot(reach, spread(solved_values)) + on_value[BLOCK:]
        left = jnp.concatenate([read_state, transition], axis=0)
        on_map = dot(left, spread(carry[0, group]))
        on_add = dot(left, spread(carry[1, group]))
        read_ref[:, at] = on_map[:BLOCK].astype(BF16)
        local_ref[:, at] = on_add[:BLOCK] + local_out
        carry[0, group] = on_map[BLOCK:]
        carry[1, group] = on_add[BLOCK:] + increment
        total_ref[0, group] = on_map[BLOCK:].astype(BF16)
        total_ref[1, group] = (on_add[BLOCK:] + increment).astype(BF16)


def block_tables(receptance, key_in, value_in, decay_in, rate_in):
    tokens, columns = receptance.shape
    width = group_width(columns)
    groups = columns // width
    rows = pl.BlockSpec((BLOCK, columns), lambda b: (b, 0))
    return pl.pallas_call(
        tables_kernel,
        grid=(tokens // BLOCK,),
        in_specs=[rows] * 5,
        out_specs=[rows, rows, pl.BlockSpec((2, groups, HD, width), lambda b: (0, 0, 0, 0))],
        out_shape=[
            jax.ShapeDtypeStruct((tokens, columns), BF16),
            jax.ShapeDtypeStruct((tokens, columns), F32),
            jax.ShapeDtypeStruct((2, groups, HD, width), BF16),
        ],
        scratch_shapes=[pltpu.VMEM((2, groups, HD, width), F32)],
        name="tables",
    )(receptance, key_in, value_in, decay_in, rate_in)


def flip(me, bits):
    bit = 1
    while bit <= bits:
        if bits & bit:
            me = me + bit - 2 * bit * ((me // bit) % 2)
        bit *= 2
    return me


class Exchange:
    def __init__(self, count, own, slots, sems):
        me = lax.axis_index("tp")
        half = own.shape[0] // 2
        bits = [1 << b for b in range(count.bit_length() - 1)]
        self.count, self.copies, self.heads, self.relays, self.seen = count, {}, [], [], set()
        for number in range(len(bits)):
            for stream, order in enumerate((bits, bits[::-1])):
                at = pl.ds(stream * half, half)
                known = [0]
                for bit in order[:number]:
                    known += [k ^ bit for k in known]
                for from_delta in known:
                    bit = order[number]
                    key = (stream, from_delta ^ bit)
                    owner = flip(me, from_delta)
                    self.copies[key] = pltpu.make_async_remote_copy(
                        src_ref=slots.at[owner, at] if from_delta else own.at[at],
                        dst_ref=slots.at[owner, at],
                        send_sem=sems.at[0, stream, key[1]],
                        recv_sem=sems.at[1, stream, key[1]],
                        device_id={"tp": flip(me, bit)},
                        device_id_type=MESH,
                    )
                    if from_delta:
                        self.relays.append((key, from_delta))
                    else:
                        self.heads.append(key)

    def start(self):
        for key in self.heads:
            self.copies[key].start()

    def arrive(self, stream, delta):
        if (stream, delta) not in self.seen:
            self.seen.add((stream, delta))
            self.copies[stream, delta].wait_recv()

    def relay(self):
        for key, from_delta in self.relays:
            self.arrive(key[0], from_delta)
            self.copies[key].start()

    def wait(self, delta):
        for stream in (0, 1):
            self.arrive(stream, delta)

    def finish(self):
        for copy in self.copies.values():
            copy.wait_send()


def prefix(count, own_ref, outgoing, incoming, before, send_sem, recv_sem):
    me = lax.axis_index("ep")
    groups = own_ref.shape[1]
    steps = [1 << s for s in range(count.bit_length() - 1)]
    width = own_ref.shape[3]
    lane = lax.broadcasted_iota(jnp.int32, (HD, width), 1) % HD
    eye = (lane == lax.broadcasted_iota(jnp.int32, (HD, width), 0)).astype(F32)
    for group in range(groups):
        before[0, group] = eye
        before[1, group] = jnp.zeros_like(eye)
    for number, step in enumerate(steps):
        last = number == len(steps) - 1
        source = own_ref if number == 0 else outgoing.at[number - 1]
        target = incoming.at[number]
        if last:
            source, target = source.at[1], target.at[1]
        copy = pltpu.make_async_remote_copy(
            src_ref=source,
            dst_ref=target,
            send_sem=send_sem.at[number],
            recv_sem=recv_sem.at[number],
            device_id={"ep": lax.rem(me + step, count)},
            device_id_type=MESH,
        )

        @pl.when(me + step < count)
        def _():
            copy.start()

        @pl.when(me >= step)
        def _():
            copy.wait_recv()
            for group in range(groups):
                left = before[0, group]
                before[1, group] += dot(left, spread(incoming[number, 1, group]))
                if not last:
                    before[0, group] = dot(left, spread(incoming[number, 0, group]))

        if not last:
            for group in range(groups):
                left = own_ref[0, group]
                outgoing[number, 0, group] = dot(left, spread(before[0, group])).astype(BF16)
                outgoing[number, 1, group] = (
                    dot(left, spread(before[1, group])) + own_ref[1, group].astype(F32)
                ).astype(BF16)

        @pl.when(me + step < count)
        def _():
            copy.wait_send()


def experts_kernel(
    tp_count,
    ep_count,
    rows_ref,
    gate_hbm,
    up_hbm,
    down_hbm,
    share_ref,
    total_ref,
    read_ref,
    local_ref,
    gain_ref,
    weight_hbm,
    product_ref,
    result_ref,
    slots,
    hidden_slots,
    hidden,
    gate_w,
    up_w,
    down_w,
    out_w,
    gate,
    up,
    down,
    mixed,
    outgoing,
    incoming,
    before,
    send_sem,
    recv_sem,
    row_sems,
    hidden_sems,
    load_sems,
):
    me = lax.axis_index("tp")
    place = lax.axis_index("ep")
    steps = [1 << s for s in range(ep_count.bit_length() - 1)]
    bits = [1 << b for b in range(tp_count.bit_length() - 1)]
    loads = [
        pltpu.make_async_copy(source, target, load_sems.at[i])
        for i, (source, target) in enumerate(
            ((gate_hbm, gate_w), (up_hbm, up_w), (down_hbm, down_w), (weight_hbm, out_w))
        )
    ]
    for load in loads:
        load.start()
    barrier = pltpu.get_barrier_semaphore()

    def signal(axis, to):
        pl.semaphore_signal(barrier, inc=1, device_id={axis: to}, device_id_type=MESH)

    for bit in bits:
        signal("tp", flip(me, bit))
    for step in steps:
        pl.when(place + step < ep_count)(lambda: signal("ep", place + step))
        pl.when(place >= step)(lambda: signal("ep", place - step))
    peers = sum(
        jnp.where(place + step < ep_count, 1, 0) + jnp.where(place >= step, 1, 0)
        for step in steps
    )
    pl.semaphore_wait(barrier, peers + len(bits))

    exchange = Exchange(tp_count, rows_ref, slots, row_sems)
    exchange.start()
    prefix(ep_count, total_ref, outgoing, incoming, before, send_sem, recv_sem)
    part_width = rows_ref.shape[1]
    units = gate.shape[1]

    def slice_product(block, owner, first):
        at = pl.ds(pl.multiple_of(owner * part_width, part_width), part_width)
        for total, weight in ((gate, gate_w), (up, up_w)):
            product = jnp.dot(block, weight[at, :], preferred_element_type=F32)
            total[...] = product if first else total[...] + product

    loads[0].wait()
    loads[1].wait()
    exchange.relay()
    slice_product(rows_ref[...], me, True)
    columns = read_ref.shape[1]
    groups, width = total_ref.shape[1], total_ref.shape[3]
    ones = head_ones(width)
    for group in range(groups):
        at = pl.ds(group * width, width)
        heads_out = dot(read_ref[:, at], spread(before[1, group])) + local_ref[:, at]
        center = heads_out - dot_exact(heads_out, ones) / HD
        variance = dot_exact(center * center, ones) / HD
        mixed[:, at] = (center * lax.rsqrt(variance + 1.0) * gain_ref[:, at]).astype(BF16)
    for delta in range(1, tp_count):
        exchange.wait(delta)
        slice_product(slots[flip(me, delta)], flip(me, delta), False)
    hidden[...] = (jax.nn.silu(gate[...]) * up[...]).astype(BF16)
    hidden_exchange = Exchange(tp_count, hidden, hidden_slots, hidden_sems)
    hidden_exchange.start()

    def down_product(block, owner):
        at = pl.ds(pl.multiple_of(owner * units, units), units)
        return jnp.dot(block, down_w[at, :], preferred_element_type=F32)

    loads[2].wait()
    loads[3].wait()
    down[...] = down_product(hidden[...], me)
    tile = product_ref.shape[1] // 4
    for number in range(4):
        at = pl.ds(number * tile, tile)
        product_ref[:, at] = jnp.dot(
            mixed[...], out_w[:, at], preferred_element_type=F32
        ).astype(BF16)
        if number == 1:
            hidden_exchange.relay()
    for delta in range(1, tp_count):
        hidden_exchange.wait(delta)
        down[...] += down_product(hidden_slots[flip(me, delta)], flip(me, delta))
    result_ref[...] = (down[...] * share_ref[...]).astype(BF16)
    exchange.finish()
    hidden_exchange.finish()


def experts(rows, gate_w, up_w, down_w, share, total, read, local_out, gain, out_w):
    tp_count, ep_count = lax.axis_size("tp"), lax.axis_size("ep")
    row_count, part_width = rows.shape
    units, out_part = gate_w.shape[1], down_w.shape[1]
    tokens, columns = read.shape
    steps = ep_count.bit_length() - 1
    vmem = pl.BlockSpec(memory_space=pltpu.VMEM)
    hbm = pl.BlockSpec(memory_space=pl.ANY)
    return pl.pallas_call(
        functools.partial(experts_kernel, tp_count, ep_count),
        out_shape=[
            jax.ShapeDtypeStruct((tokens, out_w.shape[1]), BF16),
            jax.ShapeDtypeStruct((row_count, out_part), BF16),
        ],
        in_specs=[vmem, hbm, hbm, hbm, vmem, vmem, vmem, vmem, vmem, hbm],
        out_specs=[vmem, vmem],
        scratch_shapes=[
            pltpu.VMEM((tp_count, row_count, part_width), BF16),
            pltpu.VMEM((tp_count, row_count, units), BF16),
            pltpu.VMEM((row_count, units), BF16),
            pltpu.VMEM(gate_w.shape, BF16),
            pltpu.VMEM(up_w.shape, BF16),
            pltpu.VMEM(down_w.shape, BF16),
            pltpu.VMEM(out_w.shape, BF16),
            pltpu.VMEM((row_count, units), F32),
            pltpu.VMEM((row_count, units), F32),
            pltpu.VMEM((row_count, out_part), F32),
            pltpu.VMEM((tokens, columns), BF16),
            pltpu.VMEM((steps, *total.shape), BF16),
            pltpu.VMEM((steps, *total.shape), BF16),
            pltpu.VMEM(total.shape, F32),
            pltpu.SemaphoreType.DMA((steps,)),
            pltpu.SemaphoreType.DMA((steps,)),
            pltpu.SemaphoreType.DMA((2, 2, tp_count)),
            pltpu.SemaphoreType.DMA((2, 2, tp_count)),
            pltpu.SemaphoreType.DMA((4,)),
        ],
        compiler_params=pltpu.CompilerParams(
            collective_id=0, has_side_effects=True, vmem_limit_bytes=60 * 1024 * 1024
        ),
        name="experts",
    )(rows, gate_w, up_w, down_w, share, total, read, local_out, gain, out_w)


def scatter(product):
    return lax.psum_scatter(product, "tp", scatter_dimension=0, tiled=True)


def return_kernel(count, placed_ref, out_ref, pair_in, held, from_left, from_right, sems):
    me = lax.axis_index("ep")
    chips = count // 2
    core = lax.rem(me, 2)
    chip = me // 2
    partner = me + 1 - 2 * core
    barrier = pltpu.get_barrier_semaphore()

    def signal(to):
        pl.semaphore_signal(barrier, inc=1, device_id={"ep": to}, device_id_type=MESH)

    signal(partner)
    pl.when(chip > 0)(lambda: signal(me - 2))
    pl.when(chip < chips - 1)(lambda: signal(me + 2))
    pl.semaphore_wait(
        barrier, 1 + jnp.where(chip > 0, 1, 0) + jnp.where(chip < chips - 1, 1, 0)
    )

    half = out_ref.shape[0] // 2
    right_to = jnp.minimum(me + 2, count - 2 + core)
    left_to = jnp.maximum(me - 2, core)

    def send(source, target, kind, item, to):
        at, part = item
        rows = pl.ds(part * half, half)
        return pltpu.make_async_remote_copy(
            src_ref=source.at[rows],
            dst_ref=target.at[at, rows],
            send_sem=sems.at[kind, 0, 2 * at + part],
            recv_sem=sems.at[kind, 1, 2 * at + part],
            device_id={"ep": to},
            device_id_type=MESH,
        )

    def pair(item):
        return send(placed_ref.at[2 * item[0] + 1 - core], pair_in, 0, item, partner)

    def right(item, source=from_left):
        return send(source.at[item[0]], from_left, 1, item, right_to)

    def left(item, source=from_right):
        return send(source.at[item[0]], from_right, 2, item, left_to)

    order = []
    for step in range(chips):
        order += [at for at in (chips - 1 - step, step) if at not in order]
    items = [(at, part) for at in order for part in (0, 1)]
    for item in items:
        pair(item).start()

    def pair_sum(item):
        at, part = item
        rows = pl.ds(part * half, half)
        pair(item).wait_recv()
        held[at, rows] = (
            placed_ref[2 * at + core, rows].astype(F32) + pair_in[at, rows].astype(F32)
        ).astype(BF16)

    def forward(item, moving, hop, landing, origin):
        at, part = item
        rows = pl.ds(part * half, half)

        @pl.when(moving & origin)
        def _():
            hop(item, held).start()

        @pl.when(moving & jnp.logical_not(origin))
        def _():
            relay = hop(item)
            relay.wait_recv()
            landing[at, rows] = (
                landing[at, rows].astype(F32) + held[at, rows].astype(F32)
            ).astype(BF16)
            relay.start()

    ready = []
    for step in range(chips):
        for at in (chips - 1 - step, step):
            if at not in ready:
                pair_sum((at, 0))
                pair_sum((at, 1))
                ready.append(at)
        for part in (0, 1):

            def rightward(at=chips - 1 - step, part=part):
                if at > 0:
                    forward((at, part), at > chip, right, from_left, chip == 0)

            def leftward(at=step, part=part):
                if at < chips - 1:
                    forward((at, part), at < chip, left, from_right, chip == chips - 1)

            @pl.when(chip < chips // 2)
            def _():
                rightward()
                leftward()

            @pl.when(chip >= chips // 2)
            def _():
                leftward()
                rightward()

    for at in range(chips):

        @pl.when(at == chip)
        def _():
            for part in (0, 1):
                rows = pl.ds(part * half, half)
                out_ref[rows] = held[at, rows]

                @pl.when(chip > 0)
                def _():
                    right((at, part)).wait_recv()
                    out_ref[rows] = (
                        out_ref[rows].astype(F32) + from_left[at, rows].astype(F32)
                    ).astype(BF16)

                @pl.when(chip < chips - 1)
                def _():
                    left((at, part)).wait_recv()
                    out_ref[rows] = (
                        out_ref[rows].astype(F32) + from_right[at, rows].astype(F32)
                    ).astype(BF16)

    for item in items:
        pair(item).wait_send()
        pl.when(item[0] > chip)(lambda: right(item).wait_send())
        pl.when(item[0] < chip)(lambda: left(item).wait_send())


def returned(placed):
    count, rows, width = placed.shape
    chips = count // 2
    vmem = pl.BlockSpec(memory_space=pltpu.VMEM)
    return pl.pallas_call(
        functools.partial(return_kernel, count),
        out_shape=jax.ShapeDtypeStruct((rows, width), BF16),
        in_specs=[vmem],
        out_specs=vmem,
        scratch_shapes=[pltpu.VMEM((chips, rows, width), BF16)] * 4
        + [pltpu.SemaphoreType.DMA((3, 2, 2 * chips))],
        compiler_params=pltpu.CompilerParams(collective_id=1, has_side_effects=True),
        name="return",
    )(placed)


def both_halves(
    mixer_args,
    norm_gain,
    out_weight,
    moe_in,
    ffn_gain,
    routes,
    route_weights,
    gate_weight,
    up_weight,
    down_weight,
):
    row_count, feature_count = moe_in.shape
    choose_count = routes.shape[1]
    ep_count = lax.axis_size("ep")
    tp_count = lax.axis_size("tp")
    expert_count = gate_weight.shape[0] * ep_count
    capacity = 5 * row_count * choose_count // (4 * expert_count)
    part_width = feature_count // tp_count
    row_values = moe_in.astype(F32)
    scale = lax.rsqrt(jnp.mean(row_values * row_values, axis=-1, keepdims=True) + 1.0)
    first = lax.axis_index("tp") * part_width
    piece = (
        lax.dynamic_slice_in_dim(moe_in, first, part_width, 1).astype(F32)
        * scale
        * lax.dynamic_slice_in_dim(ffn_gain, first, part_width, 0)
    ).astype(BF16)
    portion = route_weights / jnp.sum(route_weights, axis=-1, keepdims=True)
    names = jnp.arange(expert_count, dtype=jnp.int32)
    table = jnp.sum(
        jnp.where(routes[:, :, None] == names[None, None, :], portion[:, :, None], 0.0), axis=1
    )
    high = table.astype(BF16)
    low = (table - high.astype(F32)).astype(BF16)
    extra = jnp.pad(jnp.concatenate([high, low], axis=1), ((0, 0), (0, 128 - 2 * expert_count)))
    arrived = lax.all_gather(jnp.concatenate([piece, extra], axis=1), "ep")
    tables = block_tables(*mixer_args)
    arrived, (read, local_out, total) = lax.optimization_barrier((arrived, tables))
    mine = lax.axis_index("ep")
    shares = arrived[:, :, part_width:].astype(F32)
    shares = jnp.sum(
        jnp.where(
            lax.broadcasted_iota(jnp.int32, (1, 1, 128), 2) % expert_count == mine, shares, 0.0
        )
        * (lax.broadcasted_iota(jnp.int32, (1, 1, 128), 2) < 2 * expert_count),
        axis=-1,
    )
    named = shares > 0
    earlier = jnp.triu(jnp.ones((row_count, row_count), F32), 1)
    rank = jnp.dot(named.astype(F32), earlier)
    slots = jnp.arange(capacity, dtype=F32)
    chosen = (rank[:, None, :] == slots[None, :, None]) & named[:, None, :]
    onehot = chosen.astype(BF16)
    rows = jnp.einsum(
        "scr,srn->scn", onehot, arrived[:, :, :part_width], preferred_element_type=F32
    ).astype(BF16)
    slot_share = jnp.sum(jnp.where(chosen, shares[:, None, :], 0.0), axis=-1)
    product, result = experts(
        rows.reshape(ep_count * capacity, part_width),
        gate_weight[0],
        up_weight[0],
        down_weight[0],
        slot_share.reshape(ep_count * capacity, 1),
        total,
        read,
        local_out,
        norm_gain[None],
        out_weight,
    )
    placed = jnp.einsum(
        "scr,scd->srd",
        onehot,
        result.reshape(ep_count, capacity, -1),
        preferred_element_type=F32,
    ).astype(BF16)
    return scatter(product), returned(placed)


def local(
    receptance,
    key_in,
    value_in,
    decay_in,
    rate_in,
    norm_gain,
    out_weight,
    moe_in,
    ffn_gain,
    routes,
    route_weights,
    gate_weight,
    up_weight,
    down_weight,
):
    return both_halves(
        (receptance, key_in, value_in, decay_in, rate_in),
        norm_gain,
        out_weight,
        moe_in,
        ffn_gain,
        routes,
        route_weights,
        gate_weight,
        up_weight,
        down_weight,
    )


def solution(mesh):
    return jax.shard_map(
        local,
        mesh=mesh,
        in_specs=(
            P("ep", "tp"),
            P("ep", "tp"),
            P("ep", "tp"),
            P("ep", "tp"),
            P("ep", "tp"),
            P("tp"),
            P("tp", None),
            P("ep", None),
            P(),
            P("ep", None),
            P("ep", None),
            P("ep", None, "tp"),
            P("ep", None, "tp"),
            P("ep", None, "tp"),
        ),
        out_specs=(P(("ep", "tp"), None), P("ep", "tp")),
        check_vma=False,
    )
```

profile of v0, /device:TPU:9, one launch (start us, length us, event | category | flops | bytes accessed | tf_op | source)
XLA Modules:
  0.0 158.0 jit_solution(16380802345434900540)
XLA Ops:
  7.2 0.0 all-gather.3.cloned.1.call-start
  7.2 1.5 multiply_reduce_fusion
  8.7 0.7 reduce_sum.46
  9.4 0.7 broadcast_divide_fusion
  10.1 0.7 select_reduce_fusion.1
  10.8 0.1 copy.27
  11.0 0.7 dynamic_slice.7
  11.7 1.1 multiply_convert_fusion
  12.7 0.7 fusion.9
  13.5 0.0 reduce-scatter.2.cloned.1.call-start
  13.6 18.1 %tables.1 = (bf16[256,512]{1,0:T(8,128)(2,1)}, f32[256,512]{1,0:T(8,128)}, bf16[2,2,64,256]{3,2,1,0:T(8,128)(2,1)}) custom-call(bf16[256,512]{1,0:T(8,128)(2,1)} %r_ref.1, bf16[256,512]{1,0:T(8,128)(2,1)} %k_ref.1, bf16[256,512]{1,0:T(8,128)(2,1)} %v_ref.1, bf16[256,512]{1,0:T(8,128)(2,1)} %d_ref.1, bf16[256,512]{1,0:T(8,128)(2,1)} %a_ref.1), custom_call_target="tpu_custom_call" | custom-call | tf_op jit(solution)/shard_map/tables/pallas_call | solution.py:150
  31.7 15.1 %all-gather.3.cloned.1.call-done = bf16[1024,1152]{1,0:T(8,128)(2,1)} async-done(((bf16[128,1152]{1,0:T(8,128)(2,1)}), bf16[1024,1152]{1,0:T(8,128)(2,1)}) %all-gather.3.cloned.1.call-update) | async-done | bytes 2359312 | tf_op jit(solution)/shard_map/all_gather | solution.py:624
  46.7 1.2 multiply_reduce_fusion.1
  47.9 0.1 fusion.14
  48.0 3.2 %fusion.2 = bf16[8,80,1024]{2,1,0:T(8,128)(2,1)} fusion(bf16[8,128,1152]{2,1,0:T(8,128)(2,1)} %bitcast.11, f32[8,128]{1,0:T(8,128)S(1)} %fusion.14, pred[8,128]{1,0:T(8,128)(4,1)S(1)} %broadcast_compare_fusion), kind=kOutput, calls=%fused_computation.4 | convolution fusion | flops 168591360 | bytes 3412992 | tf_op jit(solution)/shard_map/scr,srn->scn/dot_general | solution.py:642
  51.2 0.2 select_reduce_fusion
  51.4 0.9 reshape.58.share_ref
  52.3 61.8 %experts.1 = (bf16[256,4096]{1,0:T(8,128)(2,1)}, bf16[640,1024]{1,0:T(8,128)(2,1)}) custom-call(bf16[640,1024]{1,0:T(8,128)(2,1)} %bitcast.9, bf16[4096,256]{1,0:T(8,128)(2,1)} %bitcast.12, bf16[4096,256]{1,0:T(8,128)(2,1)} %bitcast.13, bf16[1024,1024]{1,0:T(8,128)(2,1)} %bitcast.14, f32[640,1]{1,0:T(8,128)} %reshape.58.share_ref, ...), custom_call_target="tpu_custom_call" | custom-call | tf_op jit(solution)/shard_map/experts/pallas_call | solution.py:403
  114.1 0.0 reduce-scatter.2.cloned.1.call-update
  114.2 1.3 copy-done
  115.5 2.1 %convolution_convert_fusion.placed_ref = bf16[8,128,1024]{2,1,0:T(8,128)(2,1)} fusion(bf16[8,80,1024]{2,1,0:T(8,128)(2,1)S(1)} %bitcast.15, f32[8,128]{1,0:T(8,128)S(1)} %fusion.14, pred[8,128]{1,0:T(8,128)(4,1)S(1)} %broadcast_compare_fusion), kind=kOutput, calls=%fused_computation.3 | convolution fusion | flops 168984576 | bytes 3412992 | tf_op jit(solution)/shard_map/scr,scd->srd/dot_general | solution.py:658
  117.5 27.0 %return.1 = bf16[128,1024]{1,0:T(8,128)(2,1)} custom-call(bf16[8,128,1024]{2,1,0:T(8,128)(2,1)} %convolution_convert_fusion.placed_ref), custom_call_target="tpu_custom_call" | custom-call | tf_op jit(solution)/shard_map/return/pallas_call | solution.py:577
  144.5 5.0 %reduce-scatter.2.cloned.1.call-done = bf16[64,4096]{1,0:T(8,128)(2,1)} async-done(((bf16[256,4096]{1,0:T(8,128)(2,1)}), bf16[64,4096]{1,0:T(8,128)(2,1)}) %reduce-scatter.2.cloned.1.call-update) | async-done | bytes 524304 | tf_op jit(solution)/shard_map/reduce_scatter | solution.py:440
  149.5 1.7 %copy.29 = bf16[128,1024]{1,0:T(8,128)(2,1)} copy(bf16[128,1024]{1,0:T(8,128)(2,1)} %return.1) | data formatting | bytes 524288
  (7 shorter events, 0.1 us)
Async XLA Ops:
  7.2 39.6 %all-gather.3.cloned.1.call-start = ((), (), s32[]{:S(2)}) async-start(), calls=%async_computation.2 | async-start | bytes 2654208 | tf_op jit(solution)/shard_map/all_gather | solution.py:624
  13.5 136.0 %reduce-scatter.2.cloned.1.call-start = ((), (), s32[]{:S(2)}) async-start(), calls=%async_computation.1 | async-start | bytes 2621440 | tf_op jit(solution)/shard_map/reduce_scatter | solution.py:440
  114.1 1.3 copy-start
Sparse Core Ops, SparseCore 0:
  13.6 33.0 all-gather.2
  114.3 35.1 reduce-scatter.1
where the time goes:
time: 160 us; the launch traced here: 158 us
  Pallas kernels  107 us (67%)
  waiting for transfers between devices  20.1 us (13%)
  between operations  14.1 us (9%)
  other arithmetic  6.84 us (4%)
  matrix products  5.34 us (3%)
  local copies, waits for them, and re-layouts  4.65 us (3%)
    pallas_call x1, Pallas kernels, experts(): pl.pallas_call(functools.partial(experts_kernel, tp_count, ep_count), out...  61.8 us
    pallas_call x1, Pallas kernels, returned(): pl.pallas_call(functools.partial(return_kernel, count), out_shape=jax.Sha...  27 us
    pallas_call x1, Pallas kernels, block_tables(): pl.pallas_call(tables_kernel, grid=(tokens // BLOCK,), in_specs=[rows] *...  18.1 us
    all_gather x1, waiting for transfers between devices, both_halves(): arrived = lax.all_gather(jnp.concatenate([piece, extra], axis=1), 'ep')  15.1 us
    reduce_scatter x1, waiting for transfers between devices, scatter(): return lax.psum_scatter(product, 'tp', scatter_dimension=0, tiled=True)  4.99 us
  transfers between devices with their start and end apart: 2, of which 2 were waited for; matrix products, arithmetic and copies ran while one was open for 1% of the time, Pallas kernels for 29%

commit v1 on v0

v1 whole, which is shorter than its diff:
```python
import functools

import jax
import jax.numpy as jnp
from jax import lax
from jax.experimental import pallas as pl
from jax.experimental.pallas import tpu as pltpu
from jax.sharding import PartitionSpec as P

HD = 64
BLOCK = 64
F32 = jnp.float32
BF16 = jnp.bfloat16
MESH = pl.DeviceIdType.MESH


def dot(a, b):
    return jnp.dot(a.astype(BF16), b.astype(BF16), preferred_element_type=F32)


def dot_rows(a, b):
    return lax.dot_general(
        a.astype(BF16), b.astype(BF16), (((1,), (1,)), ((), ())), preferred_element_type=F32
    )


def dot_cols(a, b):
    return lax.dot_general(
        a.astype(BF16), b.astype(BF16), (((0,), (0,)), ((), ())), preferred_element_type=F32
    )


def halves(a):
    high = a.astype(BF16)
    return high, (a - high.astype(F32)).astype(BF16)


def dot_left(mask, b):
    high, low = halves(b)
    return dot(mask, high) + dot(mask, low)


def dot_right(a, mask):
    high, low = halves(a)
    return dot(high, mask) + dot(low, mask)


def lane_head(rows, width):
    return lax.broadcasted_iota(jnp.int32, (rows, width), 1) // HD


def spread(packed):
    rows, width = packed.shape
    packed = packed.astype(BF16)
    head = lane_head(rows, width)
    return jnp.concatenate(
        [jnp.where(head == i, packed, jnp.zeros_like(packed)) for i in range(width // HD)], axis=0
    )


def fold(square):
    width = square.shape[1]
    head = lane_head(HD, width)
    out = jnp.zeros((HD, width), F32)
    for i in range(width // HD):
        out = jnp.where(head == i, square[i * HD : (i + 1) * HD], out)
    return out


def head_ones(width):
    row = lax.broadcasted_iota(jnp.int32, (width, width), 0) // HD
    return (row == lane_head(width, width)).astype(BF16)


def group_width(columns):
    return HD * max(g for g in (4, 2, 1) if columns % (g * HD) == 0)


def tables_block(block, mix_in, read_ref, local_ref, total_ref, carry, last):
    columns = read_ref.shape[1]
    width = group_width(columns)
    row = lax.broadcasted_iota(jnp.int32, (BLOCK, width), 0)
    lane = lax.broadcasted_iota(jnp.int32, (BLOCK, width), 1) % HD
    strict = lane < row
    closed = lane <= row
    eye = (lane == row).astype(F32)
    tril = (
        lax.broadcasted_iota(jnp.int32, (BLOCK, BLOCK), 1)
        <= lax.broadcasted_iota(jnp.int32, (BLOCK, BLOCK), 0)
    ).astype(BF16)
    ones = head_ones(width)
    rows = pl.ds(block * BLOCK, BLOCK)
    for group in range(columns // width):
        at = pl.ds(group * width, width)
        readout = mix_in[0, rows, at].astype(F32)
        key = mix_in[1, rows, at].astype(F32)
        value = mix_in[2, rows, at]
        log_decay = jax.nn.sigmoid(mix_in[3, rows, at].astype(F32)) * -0.6065306597126334
        rate = jax.nn.sigmoid(mix_in[4, rows, at].astype(F32))
        unit = key * lax.rsqrt(dot_right(key * key, ones) + 1.0)
        inclusive = dot_left(tril, log_decay)
        total = inclusive[BLOCK - 1 :]
        probe = -unit * jnp.exp(inclusive - log_decay)
        removal = unit * rate
        written = key * rate
        back = jnp.exp(-inclusive)
        tail = jnp.exp(total - inclusive)
        readout = readout * jnp.exp(inclusive)
        left = jnp.concatenate([probe, readout], axis=0)
        on_removal = dot_rows(left, spread(removal * back))
        on_write = dot_rows(left, spread(written * back))
        lower = jnp.where(strict, on_removal[:BLOCK], 0.0)
        reach = jnp.where(closed, on_removal[BLOCK:], 0.0)
        lower_write = jnp.where(strict, on_write[:BLOCK], 0.0)
        reach_write = jnp.where(closed, on_write[BLOCK:], 0.0)
        value_wide = spread(value)
        on_value = dot(jnp.concatenate([lower_write, reach_write], axis=0), value_wide)
        inverse = eye + lower
        power = dot(lower, spread(lower))
        for doubling in range(BLOCK.bit_length() - 2):
            wide = spread(power)
            if doubling < BLOCK.bit_length() - 3:
                both = dot(jnp.concatenate([inverse, power], axis=0), wide)
                inverse = inverse + both[:BLOCK]
                power = both[BLOCK:]
            else:
                inverse = inverse + dot(inverse, wide)
        solved_probe = dot(inverse, spread(probe))
        solved_values = dot(inverse, spread(on_value[:BLOCK]))
        transition = eye * jnp.exp(total) + fold(dot_cols(removal * tail, solved_probe))
        increment = fold(
            dot_cols(
                jnp.concatenate([removal * tail, written * tail], axis=0),
                jnp.concatenate([solved_values.astype(BF16), value], axis=0),
            )
        )
        read_state = readout + dot(reach, spread(solved_probe))
        local_out = dot(reach, spread(solved_values)) + on_value[BLOCK:]
        if block == 0:
            new_map, new_add = transition, increment
            read_ref[rows, at] = read_state.astype(BF16)
            local_ref[rows, at] = local_out
        else:
            left = jnp.concatenate([read_state, transition], axis=0)
            on_map = dot(left, spread(carry[0, group]))
            on_add = dot(left, spread(carry[1, group]))
            read_ref[rows, at] = on_map[:BLOCK].astype(BF16)
            local_ref[rows, at] = on_add[:BLOCK] + local_out
            new_map, new_add = on_map[BLOCK:], on_add[BLOCK:] + increment
        if last:
            total_ref[0, group] = new_map.astype(BF16)
            total_ref[1, group] = new_add.astype(BF16)
        else:
            carry[0, group] = new_map
            carry[1, group] = new_add


def flip(me, bits):
    bit = 1
    while bit <= bits:
        if bits & bit:
            me = me + bit - 2 * bit * ((me // bit) % 2)
        bit *= 2
    return me


def bit_list(count):
    return [1 << b for b in range(count.bit_length() - 1)]


class Exchange:
    def __init__(self, count, slots, sems, unit):
        me = lax.axis_index("tp")
        half = slots.shape[1] // 2
        bits = bit_list(count)
        self.count, self.copies, self.heads, self.relays, self.seen = count, {}, [], [], set()
        for number in range(len(bits)):
            for stream, order in enumerate((bits, bits[::-1])):
                at = pl.ds(stream * half, half)
                known = [0]
                for bit in order[:number]:
                    known += [k ^ bit for k in known]
                for from_delta in known:
                    bit = order[number]
                    key = (stream, from_delta ^ bit)
                    owner = flip(me, from_delta)
                    self.copies[key] = pltpu.make_async_remote_copy(
                        src_ref=slots.at[owner, at],
                        dst_ref=slots.at[owner, at],
                        send_sem=sems.at[unit, 0, stream, key[1]],
                        recv_sem=sems.at[unit, 1, stream, key[1]],
                        device_id={"tp": flip(me, bit)},
                        device_id_type=MESH,
                    )
                    if from_delta:
                        self.relays.append((key, from_delta))
                    else:
                        self.heads.append(key)

    def start(self, streams=(0, 1)):
        for key in self.heads:
            if key[0] in streams:
                self.copies[key].start()

    def arrive(self, stream, delta):
        if (stream, delta) not in self.seen:
            self.seen.add((stream, delta))
            self.copies[stream, delta].wait_recv()

    def relay(self):
        for key, from_delta in self.relays:
            self.arrive(key[0], from_delta)
            self.copies[key].start()

    def wait(self, delta):
        for stream in (0, 1):
            self.arrive(stream, delta)

    def finish(self):
        for copy in self.copies.values():
            copy.wait_send()


class Prefix:
    def __init__(self, count, own, outgoing, incoming, before, sems):
        self.me, self.count = lax.axis_index("ep"), count
        self.own, self.outgoing, self.incoming, self.before = own, outgoing, incoming, before
        self.steps = bit_list(count)
        self.copies = []
        for number, step in enumerate(self.steps):
            source = own if number == 0 else outgoing.at[number - 1]
            target = incoming.at[number]
            if number == len(self.steps) - 1:
                source, target = source.at[1], target.at[1]
            self.copies.append(
                pltpu.make_async_remote_copy(
                    src_ref=source,
                    dst_ref=target,
                    send_sem=sems.at[0, number],
                    recv_sem=sems.at[1, number],
                    device_id={"ep": lax.rem(self.me + step, count)},
                    device_id_type=MESH,
                )
            )

    def begin(self):
        groups, width = self.own.shape[1], self.own.shape[3]
        lane = lax.broadcasted_iota(jnp.int32, (HD, width), 1) % HD
        eye = (lane == lax.broadcasted_iota(jnp.int32, (HD, width), 0)).astype(F32)
        for group in range(groups):
            self.before[0, group] = eye
            self.before[1, group] = jnp.zeros_like(eye)

    def send(self, number):
        pl.when(self.me + self.steps[number] < self.count)(self.copies[number].start)

    def receive(self, number):
        last = number == len(self.steps) - 1
        groups = self.own.shape[1]
        own, before, incoming = self.own, self.before, self.incoming

        @pl.when(self.me >= self.steps[number])
        def _():
            self.copies[number].wait_recv()
            for group in range(groups):
                left = before[0, group]
                before[1, group] += dot(left, spread(incoming[number, 1, group]))
                if not last:
                    before[0, group] = dot(left, spread(incoming[number, 0, group]))

        if not last:
            for group in range(groups):
                left = own[0, group]
                self.outgoing[number, 0, group] = dot(left, spread(before[0, group])).astype(BF16)
                self.outgoing[number, 1, group] = (
                    dot(left, spread(before[1, group])) + own[1, group].astype(F32)
                ).astype(BF16)

    def finish(self):
        for step, copy in zip(self.steps, self.copies):
            pl.when(self.me + step < self.count)(copy.wait_send)


class Reduce:
    def __init__(self, count, parts, landing, sems):
        self.me = lax.axis_index("tp")
        self.parts, self.landing = parts, landing
        self.half = parts.shape[2] // 2
        bits = bit_list(count)
        self.orders = (bits, bits[::-1])
        self.stages, self.copies = [], {}
        left = [list(range(count))] * 2
        for number in range(len(bits)):
            stage = []
            for stream in (0, 1):
                bit = self.orders[stream][number]
                sent = [d for d in left[stream] if d & bit]
                left[stream] = [d for d in left[stream] if not d & bit]
                at = pl.ds(stream * self.half, self.half)
                for delta in sent:
                    owner = flip(self.me, delta)
                    self.copies[stream, delta] = pltpu.make_async_remote_copy(
                        src_ref=parts.at[owner, :, at],
                        dst_ref=landing.at[delta, :, at],
                        send_sem=sems.at[0, stream, delta],
                        recv_sem=sems.at[1, stream, delta],
                        device_id={"tp": flip(self.me, bit)},
                        device_id_type=MESH,
                    )
                    stage.append((stream, delta, bit))
            self.stages.append(stage)

    def start(self, number):
        for stream, delta, _ in self.stages[number]:
            self.copies[stream, delta].start()

    def land(self, number, out=None):
        for stream, delta, bit in self.stages[number]:
            at = pl.ds(stream * self.half, self.half)
            self.copies[stream, delta].wait_recv()
            mine = flip(self.me, delta ^ bit)
            total = self.parts[mine, :, at].astype(F32) + self.landing[delta, :, at].astype(F32)
            if out is None:
                self.parts[mine, :, at] = total.astype(BF16)
            else:
                out[:, at] = total.astype(BF16)

    def finish(self):
        for copy in self.copies.values():
            copy.wait_send()


class Dispatch:
    def __init__(self, chips, tp_count, rows, info, sems, info_sems, pair_sems, pair_info):
        me = lax.axis_index("ep")
        self.tp = lax.axis_index("tp")
        self.tp_count = tp_count
        self.core, self.chip, self.chips = lax.rem(me, 2), me // 2, chips
        self.me, self.partner = me, me + 1 - 2 * self.core
        self.rows, self.info = rows, info
        self.sems, self.info_sems = sems, info_sems
        self.pair_sems, self.pair_info = pair_sems, pair_info
        self.half = rows.shape[2] // 2

    def remote(self, ref, send, recv, to):
        return pltpu.make_async_remote_copy(
            src_ref=ref,
            dst_ref=ref,
            send_sem=send,
            recv_sem=recv,
            device_id={"ep": to},
            device_id_type=MESH,
        )

    def along(self, k, half, way, to):
        to = jnp.clip(to, 0, self.chips - 1)
        ref = self.rows.at[2 * k + self.core, self.tp, pl.ds(half * self.half, self.half)]
        return self.remote(
            ref, self.sems.at[way, k, half], self.sems.at[2, k, half], 2 * to + self.core
        )

    def along_info(self, k, way, to):
        to = jnp.clip(to, 0, self.chips - 1)
        ref = self.info.at[2 * k + self.core]
        return self.remote(
            ref, self.info_sems.at[way, k], self.info_sems.at[2, k], 2 * to + self.core
        )

    def across(self, k, place):
        ref = self.rows.at[2 * k + self.core, place]
        return self.remote(
            ref, self.pair_sems.at[0, k, place], self.pair_sems.at[1, k, place], self.partner
        )

    def from_partner(self, k, place):
        ref = self.rows.at[2 * k + 1 - self.core, place]
        return self.remote(
            ref, self.pair_sems.at[0, k, place], self.pair_sems.at[1, k, place], self.partner
        )

    def across_info(self, k, other=False):
        core = 1 - self.core if other else self.core
        ref = self.info.at[2 * k + core]
        return self.remote(ref, self.pair_info.at[0, k], self.pair_info.at[1, k], self.partner)

    def sides(self):
        return (
            (self.chip + 1 < self.chips, 0, self.chip + 1),
            (self.chip > 0, 1, self.chip - 1),
        )

    def send_own(self):
        for half in (0, 1):
            for inside, way, to in self.sides():
                pl.when(inside)(self.along(self.chip, half, way, to).start)
        for place in range(self.tp_count):
            self.across(self.chip, place).start()

    def send_info(self):
        for inside, way, to in self.sides():
            pl.when(inside)(self.along_info(self.chip, way, to).start)
        self.across_info(self.chip).start()

    def onward(self, k):
        right = k < self.chip
        to = jnp.where(right, self.chip + 1, self.chip - 1)
        return (to >= 0) & (to < self.chips), jnp.where(right, 0, 1), to

    def landed(self, k, exchange):
        moving, way, to = self.onward(k)
        for half in (0, 1):
            self.along(k, half, way, to).wait_recv()
            pl.when(moving)(self.along(k, half, way, to).start)
            exchange.start((half,))
        self.across(k, self.tp).start()
        self.along_info(k, way, to).wait_recv()
        pl.when(moving)(self.along_info(k, way, to).start)
        self.across_info(k).start()

    def shared(self, k, exchange, delta):
        exchange.wait(delta)
        self.across(k, flip(self.tp, delta)).start()

    def finish(self, order):
        for half in (0, 1):
            for inside, way, to in self.sides():
                pl.when(inside)(self.along(self.chip, half, way, to).wait_send)
        for inside, way, to in self.sides():
            pl.when(inside)(self.along_info(self.chip, way, to).wait_send)
        for k in order:
            moving, way, to = self.onward(k)
            for half in (0, 1):
                pl.when(moving)(self.along(k, half, way, to).wait_send)
            pl.when(moving)(self.along_info(k, way, to).wait_send)
        for k in [self.chip] + order:
            for place in range(self.tp_count):
                self.across(k, place).wait_send()
            self.across_info(k).wait_send()


def chip_order(chip, chips):
    table = [
        sorted((k for k in range(chips) if k != at), key=lambda k: (abs(k - at), k))
        for at in range(chips)
    ]
    return [
        sum(jnp.where(chip == at, table[at][number], 0) for at in range(chips))
        for number in range(chips - 1)
    ]


class Back:
    def __init__(self, count, placed, out, pair_in, held, from_left, from_right, sems):
        me = lax.axis_index("ep")
        self.chips = count // 2
        self.core = lax.rem(me, 2)
        self.chip = me // 2
        self.partner = me + 1 - 2 * self.core
        self.half = out.shape[0] // 2
        self.right_to = jnp.minimum(me + 2, count - 2 + self.core)
        self.left_to = jnp.maximum(me - 2, self.core)
        self.placed, self.out, self.pair_in, self.held = placed, out, pair_in, held
        self.from_left, self.from_right, self.sems = from_left, from_right, sems

    def send(self, source, target, kind, item, to):
        at, part = item
        rows = pl.ds(part * self.half, self.half)
        return pltpu.make_async_remote_copy(
            src_ref=source.at[rows],
            dst_ref=target.at[at, rows],
            send_sem=self.sems.at[kind, 0, 2 * at + part],
            recv_sem=self.sems.at[kind, 1, 2 * at + part],
            device_id={"ep": to},
            device_id_type=MESH,
        )

    def pair(self, item):
        source = self.placed.at[2 * item[0] + 1 - self.core]
        return self.send(source, self.pair_in, 0, item, self.partner)

    def right(self, item, source=None):
        source = self.from_left if source is None else source
        return self.send(source.at[item[0]], self.from_left, 1, item, self.right_to)

    def left(self, item, source=None):
        source = self.from_right if source is None else source
        return self.send(source.at[item[0]], self.from_right, 2, item, self.left_to)

    def pair_sum(self, item):
        at, part = item
        rows = pl.ds(part * self.half, self.half)
        self.pair(item).wait_recv()
        self.held[at, rows] = (
            self.placed[2 * at + self.core, rows].astype(F32) + self.pair_in[at, rows].astype(F32)
        ).astype(BF16)

    def forward(self, item, moving, hop, landing, origin):
        at, part = item
        rows = pl.ds(part * self.half, self.half)

        @pl.when(moving & origin)
        def _():
            hop(item, self.held).start()

        @pl.when(moving & jnp.logical_not(origin))
        def _():
            relay = hop(item)
            relay.wait_recv()
            landing[at, rows] = (
                landing[at, rows].astype(F32) + self.held[at, rows].astype(F32)
            ).astype(BF16)
            relay.start()

    def run(self):
        chips, chip = self.chips, self.chip
        ready = []
        for step in range(chips):
            for at in (chips - 1 - step, step):
                if at not in ready:
                    self.pair_sum((at, 0))
                    self.pair_sum((at, 1))
                    ready.append(at)
            for part in (0, 1):

                def rightward(at=chips - 1 - step, part=part):
                    if at > 0:
                        self.forward(
                            (at, part), at > chip, self.right, self.from_left, chip == 0
                        )

                def leftward(at=step, part=part):
                    if at < chips - 1:
                        self.forward(
                            (at, part), at < chip, self.left, self.from_right, chip == chips - 1
                        )

                @pl.when(chip < chips // 2)
                def _():
                    rightward()
                    leftward()

                @pl.when(chip >= chips // 2)
                def _():
                    leftward()
                    rightward()

    def collect(self):
        chip, at = self.chip, self.chip
        for part in (0, 1):
            rows = pl.ds(part * self.half, self.half)
            self.out[rows] = self.held[at, rows]
            for inside, hop, landing in (
                (chip > 0, self.right, self.from_left),
                (chip < self.chips - 1, self.left, self.from_right),
            ):

                @pl.when(inside)
                def _():
                    hop((at, part)).wait_recv()
                    self.out[rows] = (
                        self.out[rows].astype(F32) + landing[at, rows].astype(F32)
                    ).astype(BF16)

    def finish(self):
        for at in range(self.chips):
            for part in (0, 1):
                item = (at, part)
                self.pair(item).wait_send()
                pl.when(at > self.chip)(self.right(item).wait_send)
                pl.when(at < self.chip)(self.left(item).wait_send)


def layer_kernel(
    tp_count,
    ep_count,
    cap,
    expert_count,
    mixer_hbm,
    gain_ref,
    weight_hbm,
    moe_hbm,
    ffn_ref,
    routes_ref,
    route_weights_ref,
    gate_hbm,
    up_hbm,
    down_hbm,
    mixer_out,
    moe_out,
    rows,
    info,
    mix_in,
    gate_w,
    up_w,
    down_w,
    out_w,
    picked,
    hidden,
    read,
    local_out,
    carry,
    total,
    outgoing,
    incoming,
    before,
    mixed,
    product,
    landing,
    placed,
    pair_in,
    held,
    from_left,
    from_right,
    load_sems,
    along_sems,
    along_info_sems,
    pair_sems,
    pair_info_sems,
    row_sems,
    hidden_sems,
    prefix_sems,
    reduce_sems,
    back_sems,
):
    tp = lax.axis_index("tp")
    place = lax.axis_index("ep")
    chips = ep_count // 2
    chip = place // 2
    steps, bits = bit_list(ep_count), bit_list(tp_count)
    row_count, part_width = rows.shape[2], rows.shape[3]
    units = gate_w.shape[1]
    moe_loads = [
        pltpu.make_async_copy(
            moe_hbm.at[:, pl.ds(t * part_width, part_width)], rows.at[place, t], load_sems.at[t]
        )
        for t in range(tp_count)
    ]
    mixer_loads = [
        pltpu.make_async_copy(source, mix_in.at[i], load_sems.at[tp_count + i])
        for i, source in enumerate(mixer_hbm)
    ]
    weight_loads = [
        pltpu.make_async_copy(source, target, load_sems.at[tp_count + 5 + i])
        for i, (source, target) in enumerate(
            ((gate_hbm, gate_w), (up_hbm, up_w), (down_hbm, down_w), (weight_hbm, out_w))
        )
    ]
    for load in moe_loads + mixer_loads + weight_loads:
        load.start()

    barrier = pltpu.get_barrier_semaphore()

    def signal(axis, to):
        pl.semaphore_signal(barrier, inc=1, device_id={axis: to}, device_id_type=MESH)

    for bit in bits:
        signal("tp", flip(tp, bit))
    for step in steps:
        pl.when(place + step < ep_count)(lambda: signal("ep", place + step))
        pl.when(place >= step)(lambda: signal("ep", place - step))
    peers = sum(
        jnp.where(place + step < ep_count, 1, 0) + jnp.where(place >= step, 1, 0)
        for step in steps
    )
    for load in moe_loads:
        load.wait()
    pl.semaphore_wait(barrier, peers + len(bits))

    dispatch = Dispatch(
        chips, tp_count, rows, info, along_sems, along_info_sems, pair_sems, pair_info_sems
    )
    order = chip_order(chip, chips)
    dispatch.send_own()

    squares = jnp.zeros((row_count, 1), F32)
    for t in range(tp_count):
        part = rows[place, t].astype(F32)
        squares += jnp.sum(part * part, axis=1, keepdims=True)
    scale = lax.rsqrt(squares / (tp_count * part_width) + 1.0)
    names = lax.broadcasted_iota(jnp.int32, (row_count, 128), 1)
    portion = route_weights_ref[...]
    portion = portion / jnp.sum(portion, axis=1, keepdims=True)
    named = jnp.zeros((row_count, 128), F32)
    table = jnp.where(names == expert_count, scale, 0.0)
    for choice in range(routes_ref.shape[1]):
        match = routes_ref[:, choice : choice + 1] == names
        named = jnp.where(match, 1.0, named)
        table = jnp.where(match, portion[:, choice : choice + 1], table)
    earlier = (
        lax.broadcasted_iota(jnp.int32, (row_count, row_count), 1)
        < lax.broadcasted_iota(jnp.int32, (row_count, row_count), 0)
    ).astype(BF16)
    rank = jnp.where(named > 0.0, dot(earlier, named), -1.0)
    info[place, :expert_count] = rank.T[:expert_count]
    info[place, expert_count : 2 * expert_count + 8] = table.T[: expert_count + 8]
    dispatch.send_info()

    slot = lax.broadcasted_iota(jnp.int32, (cap, row_count), 0).astype(F32)

    def chosen(source):
        return info[source, pl.ds(place, 1), :] == slot

    def slot_value(pick, source, index):
        return jnp.sum(
            jnp.where(pick, info[source, pl.ds(index, 1), :], 0.0), axis=1, keepdims=True
        )

    sources = [chip] + order
    exchanges = [None] + [
        Exchange(tp_count, rows.at[2 * k + dispatch.core], row_sems, n)
        for n, k in enumerate(order)
    ]
    hidden_exchanges = [
        Exchange(tp_count, hidden.at[n], hidden_sems, n) for n in range(chips)
    ]

    def gate_up(n):
        k = sources[n]
        if n > 0:
            for delta in range(1, tp_count):
                exchanges[n].wait(delta)
        for t in range(tp_count):
            dispatch.from_partner(k, t).wait_recv()
        dispatch.across_info(k, True).wait_recv()
        for core in (0, 1):
            source = 2 * k + core
            pick = chosen(source)
            factor = slot_value(pick, source, 2 * expert_count)
            onehot = pick.astype(BF16)
            for t in range(tp_count):
                part = dot(onehot, rows[source, t]) * factor * ffn_ref[t]
                picked[core * cap : (core + 1) * cap, t * part_width : (t + 1) * part_width] = (
                    part.astype(BF16)
                )
        gate = dot(picked[...], gate_w[...])
        up = dot(picked[...], up_w[...])
        hidden[n, tp] = (jax.nn.silu(gate) * up).astype(BF16)
        hidden_exchanges[n].start()

    back = Back(ep_count, placed, moe_out, pair_in, held, from_left, from_right, back_sems)

    def down(n):
        k = sources[n]
        for delta in range(1, tp_count):
            hidden_exchanges[n].wait(delta)
        result = dot(
            jnp.concatenate([hidden[n, t] for t in range(tp_count)], axis=1), down_w[...]
        )
        for core in (0, 1):
            source = 2 * k + core
            pick = chosen(source)
            share = slot_value(pick, source, expert_count + place)
            mine = result[core * cap : (core + 1) * cap] * share
            placed[source] = dot_cols(pick.astype(BF16), mine).astype(BF16)
        for part in (0, 1):
            back.pair((k, part)).start()

    def landed(n):
        dispatch.landed(sources[n], exchanges[n])

    def relay(n):
        exchanges[n].relay()
        for delta in range(1, tp_count):
            if delta & (delta - 1) == 0:
                dispatch.shared(sources[n], exchanges[n], delta)

    def share_rest(n):
        for delta in range(1, tp_count):
            if delta & (delta - 1):
                dispatch.shared(sources[n], exchanges[n], delta)

    tokens = read.shape[0]
    blocks = tokens // BLOCK

    def tables(b):
        tables_block(b, mix_in, read, local_out, total, carry, b == blocks - 1)

    prefix = Prefix(ep_count, total, outgoing, incoming, before, prefix_sems)

    weight_loads[0].wait()
    weight_loads[1].wait()
    gate_up(0)
    for load in mixer_loads:
        load.wait()
    remote = chips - 1
    landed(1)
    block = 0
    for n in range(1, remote + 1):
        if block < blocks:
            tables(block)
            block += 1
        if n + 1 <= remote:
            landed(n + 1)
        relay(n)
        if n != 2:
            hidden_exchanges[max(n - 2, 0)].relay()
        if n > 1:
            share_rest(n - 1)
            gate_up(n - 1)
    while block < blocks:
        tables(block)
        block += 1
    prefix.begin()
    prefix.send(0)
    share_rest(remote)
    gate_up(remote)
    hidden_exchanges[remote - 1].relay()
    prefix.receive(0)
    prefix.send(1)
    weight_loads[2].wait()
    down(0)
    hidden_exchanges[remote].relay()
    for number in range(1, len(steps)):
        prefix.receive(number)
        if number + 1 < len(steps):
            prefix.send(number + 1)
    for n in range(1, remote):
        down(n)

    columns = read.shape[1]
    groups, width = total.shape[1], total.shape[3]
    ones = head_ones(width)
    for group in range(groups):
        at = pl.ds(group * width, width)
        heads_out = dot(read[:, at], spread(before[1, group])) + local_out[:, at]
        center = heads_out - dot_right(heads_out, ones) / HD
        variance = dot_right(center * center, ones) / HD
        mixed[:, at] = (center * lax.rsqrt(variance + 1.0) * gain_ref[:, at]).astype(BF16)
    weight_loads[3].wait()
    out_rows = tokens // tp_count
    tile = out_w.shape[1] // 4
    for number in range(4):
        at = pl.ds(number * tile, tile)
        part = dot(mixed[...], out_w[:, at]).astype(BF16)
        for t in range(tp_count):
            product[t, :, at] = part[t * out_rows : (t + 1) * out_rows]
    reduce = Reduce(tp_count, product, landing, reduce_sems)
    reduce.start(0)
    down(remote)
    back.run()
    for number in range(len(bits)):
        last = number == len(bits) - 1
        reduce.land(number, mixer_out if last else None)
        if not last:
            reduce.start(number + 1)
    back.collect()

    dispatch.finish(order)
    for exchange in exchanges[1:] + hidden_exchanges:
        exchange.finish()
    prefix.finish()
    reduce.finish()
    back.finish()


def local(
    receptance,
    key_in,
    value_in,
    decay_in,
    rate_in,
    norm_gain,
    out_weight,
    moe_in,
    ffn_gain,
    routes,
    route_weights,
    gate_weight,
    up_weight,
    down_weight,
):
    tp_count, ep_count = lax.axis_size("tp"), lax.axis_size("ep")
    row_count, feature_count = moe_in.shape
    expert_count = gate_weight.shape[0] * ep_count
    cap = 5 * row_count * routes.shape[1] // (4 * expert_count)
    cap = -(-cap // 16) * 16
    chips = ep_count // 2
    part_width = feature_count // tp_count
    units, out_part = gate_weight.shape[2], down_weight.shape[2]
    tokens, columns = receptance.shape
    width = group_width(columns)
    groups = columns // width
    steps = ep_count.bit_length() - 1
    out_rows = tokens // tp_count
    dim = out_weight.shape[1]
    vmem = pl.BlockSpec(memory_space=pltpu.VMEM)
    hbm = pl.BlockSpec(memory_space=pl.ANY)
    state = (2, groups, HD, width)
    dma = pltpu.SemaphoreType.DMA

    def kernel(r, k, v, d, a, *refs):
        layer_kernel(tp_count, ep_count, cap, expert_count, (r, k, v, d, a), *refs)

    return pl.pallas_call(
        kernel,
        out_shape=[
            jax.ShapeDtypeStruct((out_rows, dim), BF16),
            jax.ShapeDtypeStruct((row_count, out_part), BF16),
        ],
        in_specs=[hbm] * 5 + [vmem, hbm, hbm, vmem, vmem, vmem, hbm, hbm, hbm],
        out_specs=[vmem, vmem],
        scratch_shapes=[
            pltpu.VMEM((ep_count, tp_count, row_count, part_width), BF16),
            pltpu.VMEM((ep_count, 2 * expert_count + 8, row_count), F32),
            pltpu.VMEM((5, tokens, columns), BF16),
            pltpu.VMEM((feature_count, units), BF16),
            pltpu.VMEM((feature_count, units), BF16),
            pltpu.VMEM(down_weight.shape[1:], BF16),
            pltpu.VMEM(out_weight.shape, BF16),
            pltpu.VMEM((2 * cap, feature_count), BF16),
            pltpu.VMEM((chips, tp_count, 2 * cap, units), BF16),
            pltpu.VMEM((tokens, columns), BF16),
            pltpu.VMEM((tokens, columns), F32),
            pltpu.VMEM(state, F32),
            pltpu.VMEM(state, BF16),
            pltpu.VMEM((steps, *state), BF16),
            pltpu.VMEM((steps, *state), BF16),
            pltpu.VMEM(state, F32),
            pltpu.VMEM((tokens, columns), BF16),
            pltpu.VMEM((tp_count, out_rows, dim), BF16),
            pltpu.VMEM((tp_count, out_rows, dim), BF16),
            pltpu.VMEM((ep_count, row_count, out_part), BF16),
            pltpu.VMEM((chips, row_count, out_part), BF16),
            pltpu.VMEM((chips, row_count, out_part), BF16),
            pltpu.VMEM((chips, row_count, out_part), BF16),
            pltpu.VMEM((chips, row_count, out_part), BF16),
            dma((tp_count + 9,)),
            dma((3, chips, 2)),
            dma((3, chips)),
            dma((2, chips, tp_count)),
            dma((2, chips)),
            dma((chips - 1, 2, 2, tp_count)),
            dma((chips, 2, 2, tp_count)),
            dma((2, steps)),
            dma((2, 2, tp_count)),
            dma((3, 2, 2 * chips)),
        ],
        compiler_params=pltpu.CompilerParams(
            collective_id=0, has_side_effects=True, vmem_limit_bytes=63 * 1024 * 1024
        ),
        name="layer",
    )(
        receptance,
        key_in,
        value_in,
        decay_in,
        rate_in,
        norm_gain[None],
        out_weight,
        moe_in,
        ffn_gain.reshape(tp_count, 1, part_width),
        routes,
        route_weights,
        gate_weight[0],
        up_weight[0],
        down_weight[0],
    )


def solution(mesh):
    return jax.shard_map(
        local,
        mesh=mesh,
        in_specs=(
            P("ep", "tp"),
            P("ep", "tp"),
            P("ep", "tp"),
            P("ep", "tp"),
            P("ep", "tp"),
            P("tp"),
            P("tp", None),
            P("ep", None),
            P(),
            P("ep", None),
            P("ep", None),
            P("ep", None, "tp"),
            P("ep", None, "tp"),
            P("ep", None, "tp"),
        ),
        out_specs=(P(("ep", "tp"), None), P("ep", "tp")),
        check_vma=False,
    )
```

time: 160 us -> 96 us (0.60)
  waiting for transfers between devices: 20.1 us -> 0 us
  Pallas kernels: 107 us -> 87.4 us
  between operations: 14.1 us -> 0.64 us
  other arithmetic: 6.84 us -> 0 us
  matrix products: 5.34 us -> 0 us
  local copies, waits for them, and re-layouts: 4.65 us -> 6.37 us
    pallas_call x3 -> x1, Pallas kernels: 107 us -> 87.4 us  [local(): pl.pallas_call(kernel, out_shape=[jax.ShapeDtypeStruct((out_rows, dim), B...]
    all_gather x1 -> x0, waiting for transfers between devices: 15.1 us -> none  [both_halves(): arrived = lax.all_gather(jnp.concatenate([piece, extra], axis=1), 'ep')]
    dot_general x3 -> x0, matrix products: 5.34 us -> none  [the longest x1 3.16 us: both_halves(): jnp.einsum('scr,srn->scn', onehot, arrived[:, :, :part_width], preferred_...]
    reduce_scatter x1 -> x0, waiting for transfers between devices: 4.99 us -> none  [scatter(): return lax.psum_scatter(product, 'tp', scatter_dimension=0, tiled=True)]
    reduce_sum x5 -> x0, other arithmetic: 4.3 us -> none  [the longest x1 1.52 us: both_halves(): jnp.mean(row_values * row_values, axis=-1, keepdims=True) + 1.0]
    unnamed x4, local copies, waits for them, and re-layouts: 3.08 us -> 6.37 us
  transfers between devices with their start and end apart: 2 -> 0, of which waited for: 2 -> 0; matrix products, arithmetic and copies ran while one was open for 1% -> 0% of each run, Pallas kernels for 29% -> 0%
where the time goes in v1:
time: 96 us; the launch traced here: 94.5 us
  Pallas kernels  87.4 us (91%)
  local copies, waits for them, and re-layouts  6.37 us (7%)
    pallas_call x1, Pallas kernels, local(): pl.pallas_call(kernel, out_shape=[jax.ShapeDtypeStruct((out_rows, dim), B...  87.4 us
    unnamed x4, local copies, waits for them, and re-layouts  6.37 us

profile of v1, /device:TPU:9, one launch (start us, length us, event | category | flops | bytes accessed | tf_op | source)
XLA Modules:
  0.0 94.5 jit_solution(6327696325747219382)
XLA Ops:
  0.6 1.4 %copy.16.refs_4_ = s32[128,4]{1,0:T(8,128)} copy(s32[128,4]{0,1:T(4,128)} %param.23) | data formatting | bytes 4096 | tf_op args[9]
  2.0 1.4 %copy.17.refs_5_ = f32[128,4]{1,0:T(8,128)} copy(f32[128,4]{0,1:T(4,128)} %param.24) | data formatting | bytes 4096 | tf_op args[10]
  3.5 87.4 %layer.1 = (bf16[64,4096]{1,0:T(8,128)(2,1)}, bf16[128,1024]{1,0:T(8,128)(2,1)}) custom-call(bf16[256,512]{1,0:T(8,128)(2,1)} %r.1, bf16[256,512]{1,0:T(8,128)(2,1)} %k.1, bf16[256,512]{1,0:T(8,128)(2,1)} %v.1, bf16[256,512]{1,0:T(8,128)(2,1)} %d.1, bf16[256,512]{1,0:T(8,128)(2,1)} %a.1, f32[1,512]{1,0:T(1,128)} %bitcast.9, bf16[512,4096]{1,0:T(8,128)(2,1)} %refs_1_.1, ...), custom_call_target="tpu_custom_call" | custom-call | tf_op jit(solution)/shard_map/layer/pallas_call | solution.py:894
  90.9 1.9 %copy.20 = bf16[64,4096]{1,0:T(8,128)(2,1)} copy(bf16[64,4096]{1,0:T(8,128)(2,1)} %get-tuple-element.4) | data formatting | bytes 1048576
  92.8 1.7 %copy.21 = bf16[128,1024]{1,0:T(8,128)(2,1)} copy(bf16[128,1024]{1,0:T(8,128)(2,1)} %get-tuple-element.5) | data formatting | bytes 524288

commit v2 on v1

--- a/solution.py
+++ b/solution.py
@@ -1,5 +1,3 @@
-import functools
-
 import jax
 import jax.numpy as jnp
 from jax import lax
@@ -169,12 +167,13 @@
 
 
 class Exchange:
-    def __init__(self, count, slots, sems, unit):
+    def __init__(self, count, slots, sems, unit, wide=False):
         me = lax.axis_index("tp")
         half = slots.shape[1] // 2
         bits = bit_list(count)
         self.count, self.copies, self.heads, self.relays, self.seen = count, {}, [], [], set()
-        for number in range(len(bits)):
+        self.seconds = []
+        for number in range(1 if wide else 0, len(bits)):
             for stream, order in enumerate((bits, bits[::-1])):
                 at = pl.ds(stream * half, half)
                 known = [0]
@@ -192,7 +191,9 @@
                         device_id={"tp": flip(me, bit)},
                         device_id_type=MESH,
                     )
-                    if from_delta:
+                    if wide and from_delta == order[0]:
+                        self.seconds.append(key)
+                    elif from_delta:
                         self.relays.append((key, from_delta))
                     else:
                         self.heads.append(key)
@@ -202,8 +203,12 @@
             if key[0] in streams:
                 self.copies[key].start()
 
+    def start_seconds(self):
+        for key in self.seconds:
+            self.copies[key].start()
+
     def arrive(self, stream, delta):
-        if (stream, delta) not in self.seen:
+        if (stream, delta) in self.copies and (stream, delta) not in self.seen:
             self.seen.add((stream, delta))
             self.copies[stream, delta].wait_recv()
 
@@ -331,7 +336,9 @@
 
 
 class Dispatch:
-    def __init__(self, chips, tp_count, rows, info, sems, info_sems, pair_sems, pair_info):
+    def __init__(
+        self, chips, tp_count, rows, info, extra, sems, info_sems, pair_sems, pair_info, extra_sems
+    ):
         me = lax.axis_index("ep")
         self.tp = lax.axis_index("tp")
         self.tp_count = tp_count
@@ -341,6 +348,99 @@
         self.sems, self.info_sems = sems, info_sems
         self.pair_sems, self.pair_info = pair_sems, pair_info
         self.half = rows.shape[2] // 2
+        bits = bit_list(tp_count)
+        self.seconds = [flip(self.tp, bits[0]), flip(self.tp, bits[-1])]
+        self.extra, self.extra_sems = extra, extra_sems
+        self.end = (self.chip == 0) | (self.chip == chips - 1)
+        self.last = self.last_of(self.chip)
+        self.passed = chips - 1 - self.last
+
+    def last_of(self, chip):
+        return jnp.where(chip >= self.chips // 2, 0, self.chips - 1)
+
+    def second(self, k, half):
+        return self.rows.at[
+            2 * k + self.core, self.seconds[half], pl.ds(half * self.half, self.half)
+        ]
+
+    def through(self, half):
+        return self.extra.at[pl.ds(half * self.half, self.half)]
+
+    def move(self, source, target, sender, receiver, half, to):
+        return pltpu.make_async_remote_copy(
+            src_ref=source,
+            dst_ref=target,
+            send_sem=self.extra_sems.at[0, sender, half],
+            recv_sem=self.extra_sems.at[1, receiver, half],
+            device_id={"ep": 2 * jnp.clip(to, 0, self.chips - 1) + self.core},
+            device_id_type=MESH,
+        )
+
+    def origin_moves(self):
+        to = jnp.where(self.chip == 0, 1, self.chips - 2)
+        for half in (0, 1):
+            source = self.second(self.chip, half)
+            if self.chips > 2:
+                yield self.move(source, self.through(half), 0, 0, half, to)
+            else:
+                yield self.move(source, source, 0, 1, half, to)
+
+    def away(self, k):
+        return jnp.where(k == 0, self.chip + 1, self.chip - 1)
+
+    def send_second(self):
+        @pl.when(self.end)
+        def _():
+            for move in self.origin_moves():
+                move.start()
+
+    def pass_moves(self):
+        to = self.away(self.passed)
+        final = self.last_of(to) == self.passed
+        for half in (0, 1):
+            source = self.through(half)
+            yield final, self.move(source, self.second(self.passed, half), 0, 1, half, to)
+            if self.chips > 4:
+                yield jnp.logical_not(final), self.move(source, source, 0, 0, half, to)
+
+    def passing(self):
+        if self.chips > 2:
+
+            @pl.when(jnp.logical_not(self.end))
+            def _():
+                for half in (0, 1):
+                    source = self.through(half)
+                    self.move(source, source, 0, 0, half, self.chip).wait_recv()
+                for wanted, move in self.pass_moves():
+                    pl.when(wanted)(move.start)
+
+    def last_moves(self):
+        to = self.away(self.last)
+        for half in (0, 1):
+            source = self.second(self.last, half)
+            yield (to >= 0) & (to < self.chips), self.move(source, source, 1, 1, half, to)
+
+    def take_second(self, exchange):
+        for half, (moving, move) in enumerate(self.last_moves()):
+            move.wait_recv()
+            pl.when(moving)(move.start)
+        exchange.start_seconds()
+
+    def finish_second(self):
+        @pl.when(self.end)
+        def _():
+            for move in self.origin_moves():
+                move.wait_send()
+
+        if self.chips > 2:
+
+            @pl.when(jnp.logical_not(self.end))
+            def _():
+                for wanted, move in self.pass_moves():
+                    pl.when(wanted)(move.wait_send)
+
+        for moving, move in self.last_moves():
+            pl.when(moving)(move.wait_send)
 
     def remote(self, ref, send, recv, to):
         return pltpu.make_async_remote_copy(
@@ -400,6 +500,7 @@
         for inside, way, to in self.sides():
             pl.when(inside)(self.along_info(self.chip, way, to).start)
         self.across_info(self.chip).start()
+        self.send_second()
 
     def onward(self, k):
         right = k < self.chip
@@ -422,6 +523,7 @@
         self.across(k, flip(self.tp, delta)).start()
 
     def finish(self, order):
+        self.finish_second()
         for half in (0, 1):
             for inside, way, to in self.sides():
                 pl.when(inside)(self.along(self.chip, half, way, to).wait_send)
@@ -440,7 +542,7 @@
 
 def chip_order(chip, chips):
     table = [
-        sorted((k for k in range(chips) if k != at), key=lambda k: (abs(k - at), k))
+        sorted((k for k in range(chips) if k != at), key=lambda k: (abs(k - at), abs(k - (0 if at < chips / 2 else chips - 1))))
         for at in range(chips)
     ]
     return [
@@ -511,7 +613,7 @@
             ).astype(BF16)
             relay.start()
 
-    def run(self):
+    def run(self, between):
         chips, chip = self.chips, self.chip
         ready = []
         for step in range(chips):
@@ -544,6 +646,9 @@
                     leftward()
                     rightward()
 
+            for action, *given in between.get(step, ()):
+                action(*given)
+
     def collect(self):
         chip, at = self.chip, self.chip
         for part in (0, 1):
@@ -576,19 +681,26 @@
     cap,
     expert_count,
     mixer_hbm,
-    gain_ref,
+    gain_hbm,
     weight_hbm,
     moe_hbm,
+    ffn_hbm,
+    routes_hbm,
+    route_weights_hbm,
+    gate_hbm,
+    up_hbm,
+    down_hbm,
+    mixer_hbm_out,
+    moe_hbm_out,
+    mixer_out,
+    moe_out,
+    gain_ref,
     ffn_ref,
     routes_ref,
     route_weights_ref,
-    gate_hbm,
-    up_hbm,
-    down_hbm,
-    mixer_out,
-    moe_out,
     rows,
     info,
+    extra,
     mix_in,
     gate_w,
     up_w,
@@ -616,6 +728,7 @@
     along_info_sems,
     pair_sems,
     pair_info_sems,
+    extra_sems,
     row_sems,
     hidden_sems,
     prefix_sems,
@@ -645,7 +758,18 @@
             ((gate_hbm, gate_w), (up_hbm, up_w), (down_hbm, down_w), (weight_hbm, out_w))
         )
     ]
-    for load in moe_loads + mixer_loads + weight_loads:
+    small_loads = [
+        pltpu.make_async_copy(source, target, load_sems.at[tp_count + 9 + i])
+        for i, (source, target) in enumerate(
+            (
+                (routes_hbm, routes_ref),
+                (route_weights_hbm, route_weights_ref),
+                (ffn_hbm, ffn_ref),
+                (gain_hbm, gain_ref),
+            )
+        )
+    ]
+    for load in moe_loads + small_loads + mixer_loads + weight_loads:
         load.start()
 
     barrier = pltpu.get_barrier_semaphore()
@@ -667,7 +791,16 @@
     pl.semaphore_wait(barrier, peers + len(bits))
 
     dispatch = Dispatch(
-        chips, tp_count, rows, info, along_sems, along_info_sems, pair_sems, pair_info_sems
+        chips,
+        tp_count,
+        rows,
+        info,
+        extra,
+        along_sems,
+        along_info_sems,
+        pair_sems,
+        pair_info_sems,
+        extra_sems,
     )
     order = chip_order(chip, chips)
     dispatch.send_own()
@@ -677,22 +810,24 @@
         part = rows[place, t].astype(F32)
         squares += jnp.sum(part * part, axis=1, keepdims=True)
     scale = lax.rsqrt(squares / (tp_count * part_width) + 1.0)
-    names = lax.broadcasted_iota(jnp.int32, (row_count, 128), 1)
+    for load in small_loads:
+        load.wait()
+    names = lax.broadcasted_iota(jnp.int32, (expert_count, row_count), 0)
     portion = route_weights_ref[...]
-    portion = portion / jnp.sum(portion, axis=1, keepdims=True)
-    named = jnp.zeros((row_count, 128), F32)
-    table = jnp.where(names == expert_count, scale, 0.0)
-    for choice in range(routes_ref.shape[1]):
-        match = routes_ref[:, choice : choice + 1] == names
+    portion = portion / jnp.sum(portion, axis=0, keepdims=True)
+    named = jnp.zeros((expert_count, row_count), F32)
+    table = jnp.zeros((expert_count, row_count), F32)
+    for choice in range(routes_ref.shape[0]):
+        match = routes_ref[choice : choice + 1] == names
         named = jnp.where(match, 1.0, named)
-        table = jnp.where(match, portion[:, choice : choice + 1], table)
+        table = jnp.where(match, portion[choice : choice + 1], table)
     earlier = (
-        lax.broadcasted_iota(jnp.int32, (row_count, row_count), 1)
-        < lax.broadcasted_iota(jnp.int32, (row_count, row_count), 0)
+        lax.broadcasted_iota(jnp.int32, (row_count, row_count), 0)
+        < lax.broadcasted_iota(jnp.int32, (row_count, row_count), 1)
     ).astype(BF16)
-    rank = jnp.where(named > 0.0, dot(earlier, named), -1.0)
-    info[place, :expert_count] = rank.T[:expert_count]
-    info[place, expert_count : 2 * expert_count + 8] = table.T[: expert_count + 8]
+    info[place, :expert_count] = jnp.where(named > 0.0, dot(named, earlier), -1.0)
+    info[place, expert_count : 2 * expert_count] = table
+    info[place, 2 * expert_count :] = jnp.broadcast_to(scale, (row_count, row_count)).T[:8]
     dispatch.send_info()
 
     slot = lax.broadcasted_iota(jnp.int32, (cap, row_count), 0).astype(F32)
@@ -707,7 +842,7 @@
 
     sources = [chip] + order
     exchanges = [None] + [
-        Exchange(tp_count, rows.at[2 * k + dispatch.core], row_sems, n)
+        Exchange(tp_count, rows.at[2 * k + dispatch.core], row_sems, n, n == chips - 2)
         for n, k in enumerate(order)
     ]
     hidden_exchanges = [
@@ -772,85 +907,166 @@
     tokens = read.shape[0]
     blocks = tokens // BLOCK
 
+    def relay_hidden(n):
+        hidden_exchanges[n].relay()
+
     def tables(b):
         tables_block(b, mix_in, read, local_out, total, carry, b == blocks - 1)
 
     prefix = Prefix(ep_count, total, outgoing, incoming, before, prefix_sems)
 
-    weight_loads[0].wait()
-    weight_loads[1].wait()
-    gate_up(0)
-    for load in mixer_loads:
-        load.wait()
+    def wait_loads(loads):
+        for load in loads:
+            load.wait()
+
     remote = chips - 1
-    landed(1)
-    block = 0
-    for n in range(1, remote + 1):
-        if block < blocks:
-            tables(block)
-            block += 1
-        if n + 1 <= remote:
-            landed(n + 1)
-        relay(n)
-        if n != 2:
-            hidden_exchanges[max(n - 2, 0)].relay()
-        if n > 1:
-            share_rest(n - 1)
-            gate_up(n - 1)
-    while block < blocks:
-        tables(block)
-        block += 1
-    prefix.begin()
-    prefix.send(0)
-    share_rest(remote)
-    gate_up(remote)
-    hidden_exchanges[remote - 1].relay()
-    prefix.receive(0)
-    prefix.send(1)
-    weight_loads[2].wait()
-    down(0)
-    hidden_exchanges[remote].relay()
-    for number in range(1, len(steps)):
+    last_step = len(steps) - 1
+
+    def prefix_step(number):
         prefix.receive(number)
-        if number + 1 < len(steps):
+        if number < last_step:
             prefix.send(number + 1)
-    for n in range(1, remote):
-        down(n)
-
-    columns = read.shape[1]
-    groups, width = total.shape[1], total.shape[3]
-    ones = head_ones(width)
-    for group in range(groups):
-        at = pl.ds(group * width, width)
-        heads_out = dot(read[:, at], spread(before[1, group])) + local_out[:, at]
-        center = heads_out - dot_right(heads_out, ones) / HD
-        variance = dot_right(center * center, ones) / HD
-        mixed[:, at] = (center * lax.rsqrt(variance + 1.0) * gain_ref[:, at]).astype(BF16)
-    weight_loads[3].wait()
-    out_rows = tokens // tp_count
-    tile = out_w.shape[1] // 4
-    for number in range(4):
-        at = pl.ds(number * tile, tile)
-        part = dot(mixed[...], out_w[:, at]).astype(BF16)
-        for t in range(tp_count):
-            product[t, :, at] = part[t * out_rows : (t + 1) * out_rows]
+
+    def mixer_start():
+        prefix.begin()
+        prefix.send(0)
+
+    def heads():
+        columns = read.shape[1]
+        groups, width = total.shape[1], total.shape[3]
+        ones = head_ones(width)
+        for group in range(groups):
+            at = pl.ds(group * width, width)
+            heads_out = dot(read[:, at], spread(before[1, group])) + local_out[:, at]
+            center = heads_out - dot_right(heads_out, ones) / HD
+            variance = dot_right(center * center, ones) / HD
+            mixed[:, at] = (center * lax.rsqrt(variance + 1.0) * gain_ref[:, at]).astype(BF16)
+
+    def project():
+        weight_loads[3].wait()
+        out_rows = tokens // tp_count
+        tile = out_w.shape[1] // 4
+        for number in range(4):
+            at = pl.ds(number * tile, tile)
+            part = dot(mixed[...], out_w[:, at]).astype(BF16)
+            for t in range(tp_count):
+                product[t, :, at] = part[t * out_rows : (t + 1) * out_rows]
+
     reduce = Reduce(tp_count, product, landing, reduce_sems)
-    reduce.start(0)
-    down(remote)
-    back.run()
-    for number in range(len(bits)):
+
+    out_copies = [
+        pltpu.make_async_copy(source, target, load_sems.at[tp_count + 13 + i])
+        for i, (source, target) in enumerate(
+            ((mixer_out, mixer_hbm_out), (moe_out, moe_hbm_out))
+        )
+    ]
+
+    def reduce_step(number):
         last = number == len(bits) - 1
         reduce.land(number, mixer_out if last else None)
-        if not last:
+        if last:
+            out_copies[0].start()
+        else:
             reduce.start(number + 1)
-    back.collect()
-
-    dispatch.finish(order)
-    for exchange in exchanges[1:] + hidden_exchanges:
-        exchange.finish()
-    prefix.finish()
+
+    def collect():
+        back.collect()
+        out_copies[1].start()
+
+    inner = (chip > 0) & (chip < chips - 1)
+
+    def landed_inner(n):
+        pl.when(inner)(lambda: landed(n))
+
+    def landed_outer(n):
+        pl.when(jnp.logical_not(inner))(lambda: landed(n))
+
+    def finish_dispatch():
+        dispatch.finish(order)
+        for exchange in exchanges[1:]:
+            exchange.finish()
+
+    def finish_hidden():
+        for exchange in hidden_exchanges:
+            exchange.finish()
+        prefix.finish()
+
+    def take_second():
+        dispatch.take_second(exchanges[remote])
+
+    def second_inner():
+        pl.when(inner)(take_second)
+
+    def second_outer():
+        pl.when(jnp.logical_not(inner))(take_second)
+
+    more = [(tables, b) for b in range(blocks)]
+    chain = [(prefix_step, number) for number in range(len(steps))]
+    plan = [(wait_loads, mixer_loads), *more[:1], (landed, 1)]
+    plan += [(landed_inner, 2)] * (remote > 1)
+    plan += [(wait_loads, weight_loads[:2]), (gate_up, 0), *more[1:2]]
+    plan += [(relay, 1), (dispatch.passing,)] if remote > 1 else []
+    plan += [(landed_inner, 3)] * (remote > 2)
+    plan += [(landed_outer, 2)] * (remote > 1)
+    plan += more[2:3]
+    plan += [(share_rest, 1), (gate_up, 1), (relay_hidden, 0)] if remote > 1 else []
+    plan += [(second_inner,)] * (remote == 3)
+    plan += [(landed_outer, 3)] * (remote > 2)
+    plan += [*more[3:], (mixer_start,)]
+    for n in range(2, remote):
+        if n > 2:
+            plan.append((landed, n + 1))
+        plan += [(relay, n), (share_rest, n), *chain[:1], (gate_up, n), (relay_hidden, n - 1)]
+        chain = chain[1:]
+    plan += [(second_outer,) if remote == 3 else (take_second,)]
+    plan += [*chain[:1], (relay, remote), *chain[1:], (heads,), (project,)]
+    plan += [(relay_hidden, remote - 1), (share_rest, remote), (gate_up, remote)]
+    plan += [(wait_loads, weight_loads[2:3]), (down, 0), (finish_dispatch,)]
+    plan += [(down, n) for n in range(1, remote - 1)]
+    plan += [(relay_hidden, remote), (reduce.start, 0)]
+    plan += [(down, n) for n in range(max(1, remote - 1), remote + 1)]
+    plan += [(back.run, {chips // 2: [(reduce_step, 0)]}), (finish_hidden,)]
+    plan += [(reduce_step, number) for number in range(1, len(bits))]
+    plan += [(collect,)]
+    for step, (action, *given) in enumerate(plan):
+        with jax.named_scope(f"{action.__name__}#{step}"):
+            action(*given)
+
     reduce.finish()
     back.finish()
+    for copy in out_copies:
+        copy.wait()
+
+
+def settle_kernel(*refs):
+    sems = refs[-1]
+    count = (len(refs) - 1) // 3
+    takes, puts = [], []
+    for i in range(count):
+        held = refs[2 * count + i]
+        takes.append(pltpu.make_async_copy(refs[i], held, sems.at[0, i]))
+        puts.append(pltpu.make_async_copy(held, refs[count + i], sems.at[1, i]))
+    for take in takes:
+        take.start()
+    for take, put in zip(takes, puts):
+        take.wait()
+        put.start()
+    for put in puts:
+        put.wait()
+
+
+def settle(*arrays):
+    hbm = pl.BlockSpec(memory_space=pltpu.HBM)
+    return pl.pallas_call(
+        settle_kernel,
+        out_shape=[jax.ShapeDtypeStruct(a.shape, a.dtype) for a in arrays],
+        in_specs=[hbm] * len(arrays),
+        out_specs=[hbm] * len(arrays),
+        scratch_shapes=[pltpu.VMEM(a.shape, a.dtype) for a in arrays]
+        + [pltpu.SemaphoreType.DMA((2, len(arrays)))],
+        compiler_params=pltpu.CompilerParams(vmem_limit_bytes=63 * 2**20),
+        name="settle",
+    )(*arrays)
 
 
 def local(
@@ -883,60 +1099,70 @@
     steps = ep_count.bit_length() - 1
     out_rows = tokens // tp_count
     dim = out_weight.shape[1]
-    vmem = pl.BlockSpec(memory_space=pltpu.VMEM)
-    hbm = pl.BlockSpec(memory_space=pl.ANY)
+    hbm = pl.BlockSpec(memory_space=pltpu.HBM)
     state = (2, groups, HD, width)
     dma = pltpu.SemaphoreType.DMA
 
+    buffers = [
+        pltpu.VMEM((out_rows, dim), BF16),
+        pltpu.VMEM((row_count, out_part), BF16),
+        pltpu.VMEM((1, columns), F32),
+        pltpu.VMEM((tp_count, 1, part_width), F32),
+        pltpu.VMEM((routes.shape[1], row_count), routes.dtype),
+        pltpu.VMEM((routes.shape[1], row_count), F32),
+        pltpu.VMEM((ep_count, tp_count, row_count, part_width), BF16),
+        pltpu.VMEM((ep_count, 2 * expert_count + 8, row_count), F32),
+        pltpu.VMEM((row_count, part_width), BF16),
+        pltpu.VMEM((5, tokens, columns), BF16),
+        pltpu.VMEM((feature_count, units), BF16),
+        pltpu.VMEM((feature_count, units), BF16),
+        pltpu.VMEM(down_weight.shape[1:], BF16),
+        pltpu.VMEM(out_weight.shape, BF16),
+        pltpu.VMEM((2 * cap, feature_count), BF16),
+        pltpu.VMEM((chips, tp_count, 2 * cap, units), BF16),
+        pltpu.VMEM((tokens, columns), BF16),
+        pltpu.VMEM((tokens, columns), F32),
+        pltpu.VMEM(state, F32),
+        pltpu.VMEM(state, BF16),
+        pltpu.VMEM((steps, *state), BF16),
+        pltpu.VMEM((steps, *state), BF16),
+        pltpu.VMEM(state, F32),
+        pltpu.VMEM((tokens, columns), BF16),
+        pltpu.VMEM((tp_count, out_rows, dim), BF16),
+        pltpu.VMEM((tp_count, out_rows, dim), BF16),
+        pltpu.VMEM((ep_count, row_count, out_part), BF16),
+        pltpu.VMEM((chips, row_count, out_part), BF16),
+        pltpu.VMEM((chips, row_count, out_part), BF16),
+        pltpu.VMEM((chips, row_count, out_part), BF16),
+        pltpu.VMEM((chips, row_count, out_part), BF16),
+    ]
+    sems = [
+        dma((tp_count + 15,)),
+        dma((3, chips, 2)),
+        dma((3, chips)),
+        dma((2, chips, tp_count)),
+        dma((2, chips)),
+        dma((2, 2, 2)),
+        dma((chips - 1, 2, 2, tp_count)),
+        dma((chips, 2, 2, tp_count)),
+        dma((2, steps)),
+        dma((2, 2, tp_count)),
+        dma((3, 2, 2 * chips)),
+    ]
     def kernel(r, k, v, d, a, *refs):
         layer_kernel(tp_count, ep_count, cap, expert_count, (r, k, v, d, a), *refs)
 
-    return pl.pallas_call(
+    results = pl.pallas_call(
         kernel,
         out_shape=[
             jax.ShapeDtypeStruct((out_rows, dim), BF16),
             jax.ShapeDtypeStruct((row_count, out_part), BF16),
         ],
-        in_specs=[hbm] * 5 + [vmem, hbm, hbm, vmem, vmem, vmem, hbm, hbm, hbm],
-        out_specs=[vmem, vmem],
-        scratch_shapes=[
-            pltpu.VMEM((ep_count, tp_count, row_count, part_width), BF16),
-            pltpu.VMEM((ep_count, 2 * expert_count + 8, row_count), F32),
-            pltpu.VMEM((5, tokens, columns), BF16),
-            pltpu.VMEM((feature_count, units), BF16),
-            pltpu.VMEM((feature_count, units), BF16),
-            pltpu.VMEM(down_weight.shape[1:], BF16),
-            pltpu.VMEM(out_weight.shape, BF16),
-            pltpu.VMEM((2 * cap, feature_count), BF16),
-            pltpu.VMEM((chips, tp_count, 2 * cap, units), BF16),
-            pltpu.VMEM((tokens, columns), BF16),
-            pltpu.VMEM((tokens, columns), F32),
-            pltpu.VMEM(state, F32),
-            pltpu.VMEM(state, BF16),
-            pltpu.VMEM((steps, *state), BF16),
-            pltpu.VMEM((steps, *state), BF16),
-            pltpu.VMEM(state, F32),
-            pltpu.VMEM((tokens, columns), BF16),
-            pltpu.VMEM((tp_count, out_rows, dim), BF16),
-            pltpu.VMEM((tp_count, out_rows, dim), BF16),
-            pltpu.VMEM((ep_count, row_count, out_part), BF16),
-            pltpu.VMEM((chips, row_count, out_part), BF16),
-            pltpu.VMEM((chips, row_count, out_part), BF16),
-            pltpu.VMEM((chips, row_count, out_part), BF16),
-            pltpu.VMEM((chips, row_count, out_part), BF16),
-            dma((tp_count + 9,)),
-            dma((3, chips, 2)),
-            dma((3, chips)),
-            dma((2, chips, tp_count)),
-            dma((2, chips)),
-            dma((chips - 1, 2, 2, tp_count)),
-            dma((chips, 2, 2, tp_count)),
-            dma((2, steps)),
-            dma((2, 2, tp_count)),
-            dma((3, 2, 2 * chips)),
-        ],
+        in_specs=[hbm] * 14,
+        out_specs=[hbm, hbm],
+        scratch_shapes=buffers + sems,
         compiler_params=pltpu.CompilerParams(
-            collective_id=0, has_side_effects=True, vmem_limit_bytes=63 * 1024 * 1024
+            collective_id=0, has_side_effects=True, vmem_limit_bytes=63 * 2**20
         ),
         name="layer",
     )(
@@ -949,12 +1175,13 @@
         out_weight,
         moe_in,
         ffn_gain.reshape(tp_count, 1, part_width),
-        routes,
-        route_weights,
+        routes.T,
+        route_weights.T,
         gate_weight[0],
         up_weight[0],
         down_weight[0],
     )
+    return settle(*results)
 
 
 def solution(mesh):

time: 96 us -> 87.5 us (0.911)
  local copies, waits for them, and re-layouts: 6.37 us -> 0 us
  Pallas kernels: 87.4 us -> 85.9 us
    unnamed x4 -> x0, local copies, waits for them, and re-layouts: 6.37 us -> none
    pallas_call x1, Pallas kernels: 87.4 us -> 84 us  [local(): pl.pallas_call(kernel, out_shape=[jax.ShapeDtypeStruct((out_rows, dim), B...]
    pallas_call x0 -> x1, Pallas kernels: none -> 1.95 us  [settle(): pl.pallas_call(settle_kernel, out_shape=[jax.ShapeDtypeStruct(a.shape, a....]
where the time goes in v2:
time: 87.5 us; the launch traced here: 86.7 us
  Pallas kernels  85.9 us (98%)
    pallas_call x1, Pallas kernels, local(): pl.pallas_call(kernel, out_shape=[jax.ShapeDtypeStruct((out_rows, dim), B...  84 us
    pallas_call x1, Pallas kernels, settle(): pl.pallas_call(settle_kernel, out_shape=[jax.ShapeDtypeStruct(a.shape, a....  1.95 us

profile of v2, /device:TPU:9, one launch (start us, length us, event | category | flops | bytes accessed | tf_op | source)
XLA Modules:
  0.0 86.7 jit_solution(11366871042925217166)
XLA Ops:
  0.6 84.0 %layer.1 = (bf16[64,4096]{1,0:T(8,128)(2,1)}, bf16[128,1024]{1,0:T(8,128)(2,1)}) custom-call(bf16[256,512]{1,0:T(8,128)(2,1)} %r.1, bf16[256,512]{1,0:T(8,128)(2,1)} %k.1, bf16[256,512]{1,0:T(8,128)(2,1)} %v.1, bf16[256,512]{1,0:T(8,128)(2,1)} %d.1, bf16[256,512]{1,0:T(8,128)(2,1)} %a.1, f32[1,512]{1,0:T(1,128)} %bitcast.11, bf16[512,4096]{1,0:T(8,128)(2,1)} %refs_1_.1, ...), custom_call_target="tpu_custom_call" | custom-call | tf_op jit(solution)/shard_map/layer/pallas_call | solution.py:1155
  84.6 2.0 %settle.1 = (bf16[64,4096]{1,0:T(8,128)(2,1)}, bf16[128,1024]{1,0:T(8,128)(2,1)}) custom-call(bf16[64,4096]{1,0:T(8,128)(2,1)} %get-tuple-element.4.refs_0_, bf16[128,1024]{1,0:T(8,128)(2,1)} %get-tuple-element.5.refs_1_), custom_call_target="tpu_custom_call" | custom-call | tf_op jit(solution)/shard_map/settle/pallas_call | solution.py:1060

commit v3 on v2

--- a/solution.py
+++ b/solution.py
@@ -172,6 +172,15 @@
         half = slots.shape[1] // 2
         bits = bit_list(count)
         self.count, self.copies, self.heads, self.relays, self.seen = count, {}, [], [], set()
+        whole = slots.at[pl.ds(0, count - 2 if wide else count - 1)]
+        self.sent = pltpu.make_async_remote_copy(
+            src_ref=whole,
+            dst_ref=whole,
+            send_sem=sems.at[unit, 2 * (count - 1)],
+            recv_sem=sems.at[unit, 0],
+            device_id={"tp": flip(me, bits[0])},
+            device_id_type=MESH,
+        )
         self.seconds = []
         for number in range(1 if wide else 0, len(bits)):
             for stream, order in enumerate((bits, bits[::-1])):
@@ -186,8 +195,8 @@
                     self.copies[key] = pltpu.make_async_remote_copy(
                         src_ref=slots.at[owner, at],
                         dst_ref=slots.at[owner, at],
-                        send_sem=sems.at[unit, 0, stream, key[1]],
-                        recv_sem=sems.at[unit, 1, stream, key[1]],
+                        send_sem=sems.at[unit, 2 * (count - 1)],
+                        recv_sem=sems.at[unit, stream * (count - 1) + key[1] - 1],
                         device_id={"tp": flip(me, bit)},
                         device_id_type=MESH,
                     )
@@ -222,8 +231,7 @@
             self.arrive(stream, delta)
 
     def finish(self):
-        for copy in self.copies.values():
-            copy.wait_send()
+        self.sent.wait_send()
 
 
 class Prefix:
@@ -292,13 +300,13 @@
         self.parts, self.landing = parts, landing
         self.half = parts.shape[2] // 2
         bits = bit_list(count)
-        self.orders = (bits, bits[::-1])
-        self.stages, self.copies = [], {}
+        orders = (bits, bits[::-1])
+        self.stages, self.finals, self.copies = [], [], {}
         left = [list(range(count))] * 2
         for number in range(len(bits)):
-            stage = []
+            passed, finals = [], []
             for stream in (0, 1):
-                bit = self.orders[stream][number]
+                bit = orders[stream][number]
                 sent = [d for d in left[stream] if d & bit]
                 left[stream] = [d for d in left[stream] if not d & bit]
                 at = pl.ds(stream * self.half, self.half)
@@ -307,28 +315,41 @@
                     self.copies[stream, delta] = pltpu.make_async_remote_copy(
                         src_ref=parts.at[owner, :, at],
                         dst_ref=landing.at[delta, :, at],
-                        send_sem=sems.at[0, stream, delta],
-                        recv_sem=sems.at[1, stream, delta],
+                        send_sem=sems.at[0, stream, delta - 1],
+                        recv_sem=sems.at[1, stream, delta - 1],
                         device_id={"tp": flip(self.me, bit)},
                         device_id_type=MESH,
                     )
-                    stage.append((stream, delta, bit))
-            self.stages.append(stage)
-
-    def start(self, number):
+                    (finals if delta == bit else passed).append((stream, delta, bit))
+            self.stages.append(passed)
+            self.finals.append(finals)
+
+    def start_passed(self, number):
         for stream, delta, _ in self.stages[number]:
             self.copies[stream, delta].start()
 
-    def land(self, number, out=None):
+    def start_finals(self, number):
+        for stream, delta, _ in self.finals[number]:
+            self.copies[stream, delta].start()
+
+    def land(self, number):
         for stream, delta, bit in self.stages[number]:
             at = pl.ds(stream * self.half, self.half)
             self.copies[stream, delta].wait_recv()
             mine = flip(self.me, delta ^ bit)
             total = self.parts[mine, :, at].astype(F32) + self.landing[delta, :, at].astype(F32)
-            if out is None:
-                self.parts[mine, :, at] = total.astype(BF16)
-            else:
-                out[:, at] = total.astype(BF16)
+            self.parts[mine, :, at] = total.astype(BF16)
+
+    def last(self, out):
+        for stream in (0, 1):
+            at = pl.ds(stream * self.half, self.half)
+            total = self.parts[self.me, :, at].astype(F32)
+            for finals in self.finals:
+                for owner, delta, _ in finals:
+                    if owner == stream:
+                        self.copies[stream, delta].wait_recv()
+                        total += self.landing[delta, :, at].astype(F32)
+            out[:, at] = total.astype(BF16)
 
     def finish(self):
         for copy in self.copies.values():
@@ -468,15 +489,11 @@
 
     def across(self, k, place):
         ref = self.rows.at[2 * k + self.core, place]
-        return self.remote(
-            ref, self.pair_sems.at[0, k, place], self.pair_sems.at[1, k, place], self.partner
-        )
-
-    def from_partner(self, k, place):
-        ref = self.rows.at[2 * k + 1 - self.core, place]
-        return self.remote(
-            ref, self.pair_sems.at[0, k, place], self.pair_sems.at[1, k, place], self.partner
-        )
+        return self.remote(ref, self.pair_sems.at[0, k], self.pair_sems.at[1, k], self.partner)
+
+    def all_across(self, k, other=False):
+        ref = self.rows.at[2 * k + (1 - self.core if other else self.core)]
+        return self.remote(ref, self.pair_sems.at[0, k], self.pair_sems.at[1, k], self.partner)
 
     def across_info(self, k, other=False):
         core = 1 - self.core if other else self.core
@@ -535,8 +552,7 @@
                 pl.when(moving)(self.along(k, half, way, to).wait_send)
             pl.when(moving)(self.along_info(k, way, to).wait_send)
         for k in [self.chip] + order:
-            for place in range(self.tp_count):
-                self.across(k, place).wait_send()
+            self.all_across(k).wait_send()
             self.across_info(k).wait_send()
 
 
@@ -570,15 +586,21 @@
         return pltpu.make_async_remote_copy(
             src_ref=source.at[rows],
             dst_ref=target.at[at, rows],
-            send_sem=self.sems.at[kind, 0, 2 * at + part],
-            recv_sem=self.sems.at[kind, 1, 2 * at + part],
+            send_sem=self.sems.at[2 * self.chips + 2 * at + part],
+            recv_sem=self.sems.at[2 * self.chips * (kind + 1) + 2 * at + part],
             device_id={"ep": to},
             device_id_type=MESH,
         )
 
-    def pair(self, item):
-        source = self.placed.at[2 * item[0] + 1 - self.core]
-        return self.send(source, self.pair_in, 0, item, self.partner)
+    def pair(self, at):
+        return pltpu.make_async_remote_copy(
+            src_ref=self.placed.at[2 * at + 1 - self.core],
+            dst_ref=self.pair_in.at[at],
+            send_sem=self.sems.at[at],
+            recv_sem=self.sems.at[self.chips + at],
+            device_id={"ep": self.partner},
+            device_id_type=MESH,
+        )
 
     def right(self, item, source=None):
         source = self.from_left if source is None else source
@@ -588,23 +610,17 @@
         source = self.from_right if source is None else source
         return self.send(source.at[item[0]], self.from_right, 2, item, self.left_to)
 
-    def pair_sum(self, item):
+    def pair_sum(self, at):
+        self.pair(at).wait_recv()
+        self.held[at] = (
+            self.placed[2 * at + self.core].astype(F32) + self.pair_in[at].astype(F32)
+        ).astype(BF16)
+
+    def forward(self, item, moving, hop, landing):
         at, part = item
         rows = pl.ds(part * self.half, self.half)
-        self.pair(item).wait_recv()
-        self.held[at, rows] = (
-            self.placed[2 * at + self.core, rows].astype(F32) + self.pair_in[at, rows].astype(F32)
-        ).astype(BF16)
-
-    def forward(self, item, moving, hop, landing, origin):
-        at, part = item
-        rows = pl.ds(part * self.half, self.half)
-
-        @pl.when(moving & origin)
-        def _():
-            hop(item, self.held).start()
-
-        @pl.when(moving & jnp.logical_not(origin))
+
+        @pl.when(moving)
         def _():
             relay = hop(item)
             relay.wait_recv()
@@ -613,44 +629,55 @@
             ).astype(BF16)
             relay.start()
 
-    def run(self, between):
+    def origin(self, at):
+        self.pair_sum(at)
+        for part in (0, 1):
+            item = (at, part)
+            pl.when(self.chip == 0)(self.right(item, self.held).start)
+            pl.when(self.chip > 0)(self.left(item, self.held).start)
+
+    def run(self):
         chips, chip = self.chips, self.chip
-        ready = []
-        for step in range(chips):
-            for at in (chips - 1 - step, step):
-                if at not in ready:
-                    self.pair_sum((at, 0))
-                    self.pair_sum((at, 1))
-                    ready.append(at)
-            for part in (0, 1):
-
-                def rightward(at=chips - 1 - step, part=part):
-                    if at > 0:
-                        self.forward(
-                            (at, part), at > chip, self.right, self.from_left, chip == 0
-                        )
-
-                def leftward(at=step, part=part):
-                    if at < chips - 1:
-                        self.forward(
-                            (at, part), at < chip, self.left, self.from_right, chip == chips - 1
-                        )
-
-                @pl.when(chip < chips // 2)
-                def _():
-                    rightward()
-                    leftward()
-
-                @pl.when(chip >= chips // 2)
-                def _():
-                    leftward()
-                    rightward()
-
-            for action, *given in between.get(step, ()):
-                action(*given)
+        order = [1, *range(chips - 1, 1, -1)]
+        ready = set()
+
+        def summed(at):
+            if at not in ready:
+                ready.add(at)
+                self.pair_sum(at)
+
+        def step(near, number):
+            part = number % 2
+            right_at = order[number // 2]
+            left_at = chips - 1 - right_at
+
+            def rightward():
+                self.forward((right_at, part), right_at > chip, self.right, self.from_left)
+
+            def leftward():
+                self.forward((left_at, part), left_at < chip, self.left, self.from_right)
+
+            first, second = (rightward, leftward) if near else (leftward, rightward)
+            pl.when(chip < chips // 2)(first)
+            pl.when(chip >= chips // 2)(second)
+
+        lead = 2
+        items = 2 * len(order)
+        for number in range(items + lead):
+            if number < items:
+                summed(order[number // 2])
+                summed(chips - 1 - order[number // 2])
+                step(True, number)
+            if number >= lead:
+                step(False, number - lead)
 
     def collect(self):
         chip, at = self.chip, self.chip
+
+        @pl.when((chip == 0) | (chip == self.chips - 1))
+        def _():
+            self.pair_sum(at)
+
         for part in (0, 1):
             rows = pl.ds(part * self.half, self.half)
             self.out[rows] = self.held[at, rows]
@@ -668,9 +695,9 @@
 
     def finish(self):
         for at in range(self.chips):
+            self.pair(at).wait_send()
             for part in (0, 1):
                 item = (at, part)
-                self.pair(item).wait_send()
                 pl.when(at > self.chip)(self.right(item).wait_send)
                 pl.when(at < self.chip)(self.left(item).wait_send)
 
@@ -744,22 +771,22 @@
     units = gate_w.shape[1]
     moe_loads = [
         pltpu.make_async_copy(
-            moe_hbm.at[:, pl.ds(t * part_width, part_width)], rows.at[place, t], load_sems.at[t]
+            moe_hbm.at[:, pl.ds(t * part_width, part_width)], rows.at[place, t], load_sems.at[0]
         )
         for t in range(tp_count)
     ]
     mixer_loads = [
-        pltpu.make_async_copy(source, mix_in.at[i], load_sems.at[tp_count + i])
+        pltpu.make_async_copy(source, mix_in.at[i], load_sems.at[1])
         for i, source in enumerate(mixer_hbm)
     ]
     weight_loads = [
-        pltpu.make_async_copy(source, target, load_sems.at[tp_count + 5 + i])
+        pltpu.make_async_copy(source, target, load_sems.at[2 + i])
         for i, (source, target) in enumerate(
             ((gate_hbm, gate_w), (up_hbm, up_w), (down_hbm, down_w), (weight_hbm, out_w))
         )
     ]
     small_loads = [
-        pltpu.make_async_copy(source, target, load_sems.at[tp_count + 9 + i])
+        pltpu.make_async_copy(source, target, load_sems.at[6 + i])
         for i, (source, target) in enumerate(
             (
                 (routes_hbm, routes_ref),
@@ -786,8 +813,7 @@
         jnp.where(place + step < ep_count, 1, 0) + jnp.where(place >= step, 1, 0)
         for step in steps
     )
-    for load in moe_loads:
-        load.wait()
+    pltpu.make_async_copy(rows.at[place], rows.at[place], load_sems.at[0]).wait()
     pl.semaphore_wait(barrier, peers + len(bits))
 
     dispatch = Dispatch(
@@ -854,8 +880,7 @@
         if n > 0:
             for delta in range(1, tp_count):
                 exchanges[n].wait(delta)
-        for t in range(tp_count):
-            dispatch.from_partner(k, t).wait_recv()
+        dispatch.all_across(k, True).wait_recv()
         dispatch.across_info(k, True).wait_recv()
         for core in (0, 1):
             source = 2 * k + core
@@ -887,8 +912,7 @@
             share = slot_value(pick, source, expert_count + place)
             mine = result[core * cap : (core + 1) * cap] * share
             placed[source] = dot_cols(pick.astype(BF16), mine).astype(BF16)
-        for part in (0, 1):
-            back.pair((k, part)).start()
+        back.pair(k).start()
 
     def landed(n):
         dispatch.landed(sources[n], exchanges[n])
@@ -955,19 +979,35 @@
     reduce = Reduce(tp_count, product, landing, reduce_sems)
 
     out_copies = [
-        pltpu.make_async_copy(source, target, load_sems.at[tp_count + 13 + i])
+        pltpu.make_async_copy(source, target, load_sems.at[10 + i])
         for i, (source, target) in enumerate(
             ((mixer_out, mixer_hbm_out), (moe_out, moe_hbm_out))
         )
     ]
 
-    def reduce_step(number):
-        last = number == len(bits) - 1
-        reduce.land(number, mixer_out if last else None)
-        if last:
-            out_copies[0].start()
-        else:
-            reduce.start(number + 1)
+    def reduce_pass():
+        for number in range(len(bits) - 1):
+            reduce.land(number)
+            reduce.start_passed(number + 1)
+            reduce.start_finals(number + 1)
+
+    def reduce_last():
+        reduce.last(mixer_out)
+        out_copies[0].start()
+
+    def origin(n):
+        pl.when(jnp.logical_not(inner))(lambda: back.origin(sources[n]))
+
+    def run():
+        pl.when(inner)(back.run)
+
+    def relay_inner(n):
+        seen = set(exchanges[n].seen)
+        pl.when(inner)(lambda: relay(n))
+        exchanges[n].seen = seen
+
+    def relay_outer(n):
+        pl.when(jnp.logical_not(inner))(lambda: relay(n))
 
     def collect():
         back.collect()
@@ -1002,32 +1042,40 @@
 
     more = [(tables, b) for b in range(blocks)]
     chain = [(prefix_step, number) for number in range(len(steps))]
-    plan = [(wait_loads, mixer_loads), *more[:1], (landed, 1)]
+    all_mixer = pltpu.make_async_copy(mix_in, mix_in, load_sems.at[1])
+    plan = [(wait_loads, [all_mixer]), *more[:1], (landed, 1)]
     plan += [(landed_inner, 2)] * (remote > 1)
     plan += [(wait_loads, weight_loads[:2]), (gate_up, 0), *more[1:2]]
     plan += [(relay, 1), (dispatch.passing,)] if remote > 1 else []
     plan += [(landed_inner, 3)] * (remote > 2)
     plan += [(landed_outer, 2)] * (remote > 1)
     plan += more[2:3]
-    plan += [(share_rest, 1), (gate_up, 1), (relay_hidden, 0)] if remote > 1 else []
     plan += [(second_inner,)] * (remote == 3)
+    plan += [(share_rest, 1)] if remote > 1 else []
+    plan += [(relay_inner, 2)] if remote > 2 else []
+    plan += [(gate_up, 1), (relay_hidden, 0)] if remote > 1 else []
     plan += [(landed_outer, 3)] * (remote > 2)
     plan += [*more[3:], (mixer_start,)]
     for n in range(2, remote):
         if n > 2:
             plan.append((landed, n + 1))
-        plan += [(relay, n), (share_rest, n), *chain[:1], (gate_up, n), (relay_hidden, n - 1)]
+        plan.append((relay_outer if n == 2 else relay, n))
+        plan += [(second_outer,)] * (remote == 3)
+        plan += [(share_rest, n), *chain[:1], (gate_up, n), (relay_hidden, n - 1)]
         chain = chain[1:]
-    plan += [(second_outer,) if remote == 3 else (take_second,)]
-    plan += [*chain[:1], (relay, remote), *chain[1:], (heads,), (project,)]
-    plan += [(relay_hidden, remote - 1), (share_rest, remote), (gate_up, remote)]
-    plan += [(wait_loads, weight_loads[2:3]), (down, 0), (finish_dispatch,)]
-    plan += [(down, n) for n in range(1, remote - 1)]
-    plan += [(relay_hidden, remote), (reduce.start, 0)]
-    plan += [(down, n) for n in range(max(1, remote - 1), remote + 1)]
-    plan += [(back.run, {chips // 2: [(reduce_step, 0)]}), (finish_hidden,)]
-    plan += [(reduce_step, number) for number in range(1, len(bits))]
-    plan += [(collect,)]
+    plan += [(take_second,)] * (remote != 3)
+    plan += [*chain[:1], (relay, remote), *chain[1:]]
+    plan += [(share_rest, remote), (gate_up, remote), (relay_hidden, remote - 1), (heads,)]
+    plan += [(wait_loads, weight_loads[2:3])]
+    plan += [(down, 1)] if remote > 1 else []
+    plan += [(project,)]
+    plan += [(origin, 1)] if remote > 1 else []
+    plan += [(relay_hidden, remote), (reduce.start_passed, 0), (reduce.start_finals, 0)]
+    plan += [(finish_dispatch,)]
+    plan += [(down, n) for n in range(2, remote)]
+    plan += [(down, 0), (down, remote)]
+    plan += [(origin, n) for n in [remote, *range(remote - 1, 1, -1)]]
+    plan += [(reduce_pass,), (run,), (finish_hidden,), (reduce_last,), (collect,)]
     for step, (action, *given) in enumerate(plan):
         with jax.named_scope(f"{action.__name__}#{step}"):
             action(*given)
@@ -1137,17 +1185,17 @@
         pltpu.VMEM((chips, row_count, out_part), BF16),
     ]
     sems = [
-        dma((tp_count + 15,)),
+        dma((12,)),
         dma((3, chips, 2)),
         dma((3, chips)),
-        dma((2, chips, tp_count)),
+        dma((2, chips)),
         dma((2, chips)),
         dma((2, 2, 2)),
-        dma((chips - 1, 2, 2, tp_count)),
-        dma((chips, 2, 2, tp_count)),
+        dma((chips - 1, 2 * tp_count - 1)),
+        dma((chips, 2 * tp_count - 1)),
         dma((2, steps)),
-        dma((2, 2, tp_count)),
-        dma((3, 2, 2 * chips)),
+        dma((2, 2, tp_count - 1)),
+        dma((8 * chips,)),
     ]
     def kernel(r, k, v, d, a, *refs):
         layer_kernel(tp_count, ep_count, cap, expert_count, (r, k, v, d, a), *refs)

time: 87.5 us -> 80 us (0.914)
  Pallas kernels: 85.9 us -> 78.1 us
    pallas_call x1, Pallas kernels: 84 us -> 76.1 us  [local(): pl.pallas_call(kernel, out_shape=[jax.ShapeDtypeStruct((out_rows, dim), B...]
where the time goes in v3:
time: 80 us; the launch traced here: 78.9 us
  Pallas kernels  78.1 us (98%)
  between operations  0.8 us (1%)
    pallas_call x1, Pallas kernels, local(): pl.pallas_call(kernel, out_shape=[jax.ShapeDtypeStruct((out_rows, dim), B...  76.1 us
    pallas_call x1, Pallas kernels, settle(): pl.pallas_call(settle_kernel, out_shape=[jax.ShapeDtypeStruct(a.shape, a....  1.95 us

profile of v3, /device:TPU:9, one launch (start us, length us, event | category | flops | bytes accessed | tf_op | source)
XLA Modules:
  0.0 78.9 jit_solution(1121971909949684874)
XLA Ops:
  0.6 76.1 %layer.1 = (bf16[64,4096]{1,0:T(8,128)(2,1)}, bf16[128,1024]{1,0:T(8,128)(2,1)}) custom-call(bf16[256,512]{1,0:T(8,128)(2,1)} %r.1, bf16[256,512]{1,0:T(8,128)(2,1)} %k.1, bf16[256,512]{1,0:T(8,128)(2,1)} %v.1, bf16[256,512]{1,0:T(8,128)(2,1)} %d.1, bf16[256,512]{1,0:T(8,128)(2,1)} %a.1, f32[1,512]{1,0:T(1,128)} %bitcast.11, bf16[512,4096]{1,0:T(8,128)(2,1)} %refs_1_.1, ...), custom_call_target="tpu_custom_call" | custom-call | tf_op jit(solution)/shard_map/layer/pallas_call | solution.py:1203
  76.8 2.0 %settle.1 = (bf16[64,4096]{1,0:T(8,128)(2,1)}, bf16[128,1024]{1,0:T(8,128)(2,1)}) custom-call(bf16[64,4096]{1,0:T(8,128)(2,1)} %get-tuple-element.4.refs_0_, bf16[128,1024]{1,0:T(8,128)(2,1)} %get-tuple-element.5.refs_1_), custom_call_target="tpu_custom_call" | custom-call | tf_op jit(solution)/shard_map/settle/pallas_call | solution.py:1108

commit v4 on v3

--- a/solution.py
+++ b/solution.py
@@ -1,3 +1,5 @@
+import itertools
+
 import jax
 import jax.numpy as jnp
 from jax import lax
@@ -574,7 +576,8 @@
         self.core = lax.rem(me, 2)
         self.chip = me // 2
         self.partner = me + 1 - 2 * self.core
-        self.half = out.shape[0] // 2
+        self.parts = 4
+        self.half = out.shape[0] // self.parts
         self.right_to = jnp.minimum(me + 2, count - 2 + self.core)
         self.left_to = jnp.maximum(me - 2, self.core)
         self.placed, self.out, self.pair_in, self.held = placed, out, pair_in, held
@@ -586,8 +589,8 @@
         return pltpu.make_async_remote_copy(
             src_ref=source.at[rows],
             dst_ref=target.at[at, rows],
-            send_sem=self.sems.at[2 * self.chips + 2 * at + part],
-            recv_sem=self.sems.at[2 * self.chips * (kind + 1) + 2 * at + part],
+            send_sem=self.sems.at[2 * self.chips + self.parts * at + part],
+            recv_sem=self.sems.at[self.chips * (2 + self.parts * kind) + self.parts * at + part],
             device_id={"ep": to},
             device_id_type=MESH,
         )
@@ -631,14 +634,13 @@
 
     def origin(self, at):
         self.pair_sum(at)
-        for part in (0, 1):
+        for part in range(self.parts):
             item = (at, part)
             pl.when(self.chip == 0)(self.right(item, self.held).start)
             pl.when(self.chip > 0)(self.left(item, self.held).start)
 
-    def run(self):
-        chips, chip = self.chips, self.chip
-        order = [1, *range(chips - 1, 1, -1)]
+    def relays(self):
+        chips, chip, parts = self.chips, self.chip, self.parts
         ready = set()
 
         def summed(at):
@@ -647,8 +649,8 @@
                 self.pair_sum(at)
 
         def step(near, number):
-            part = number % 2
-            right_at = order[number // 2]
+            part = number % parts
+            right_at = 1 + number // parts
             left_at = chips - 1 - right_at
 
             def rightward():
@@ -661,15 +663,15 @@
             pl.when(chip < chips // 2)(first)
             pl.when(chip >= chips // 2)(second)
 
-        lead = 2
-        items = 2 * len(order)
-        for number in range(items + lead):
+        items = parts * (chips - 1)
+        for number in range(items + parts):
             if number < items:
-                summed(order[number // 2])
-                summed(chips - 1 - order[number // 2])
+                summed(1 + number // parts)
+                summed(chips - 2 - number // parts)
                 step(True, number)
-            if number >= lead:
-                step(False, number - lead)
+            if number >= parts:
+                step(False, number - parts)
+            yield
 
     def collect(self):
         chip, at = self.chip, self.chip
@@ -678,7 +680,7 @@
         def _():
             self.pair_sum(at)
 
-        for part in (0, 1):
+        for part in range(self.parts):
             rows = pl.ds(part * self.half, self.half)
             self.out[rows] = self.held[at, rows]
             for inside, hop, landing in (
@@ -696,7 +698,7 @@
     def finish(self):
         for at in range(self.chips):
             self.pair(at).wait_send()
-            for part in (0, 1):
+            for part in range(self.parts):
                 item = (at, part)
                 pl.when(at > self.chip)(self.right(item).wait_send)
                 pl.when(at < self.chip)(self.left(item).wait_send)
@@ -998,8 +1000,13 @@
     def origin(n):
         pl.when(jnp.logical_not(inner))(lambda: back.origin(sources[n]))
 
-    def run():
-        pl.when(inner)(back.run)
+    relays = back.relays()
+
+    def run(count):
+        @pl.when(inner)
+        def _():
+            for _ in itertools.islice(relays, count):
+                pass
 
     def relay_inner(n):
         seen = set(exchanges[n].seen)
@@ -1054,28 +1061,27 @@
     plan += [(share_rest, 1)] if remote > 1 else []
     plan += [(relay_inner, 2)] if remote > 2 else []
     plan += [(gate_up, 1), (relay_hidden, 0)] if remote > 1 else []
-    plan += [(landed_outer, 3)] * (remote > 2)
+    plan += [(landed_outer, 3), (relay_outer, 2)] if remote > 2 else []
     plan += [*more[3:], (mixer_start,)]
+    plan += [(second_outer,)] * (remote == 3)
     for n in range(2, remote):
         if n > 2:
-            plan.append((landed, n + 1))
-        plan.append((relay_outer if n == 2 else relay, n))
-        plan += [(second_outer,)] * (remote == 3)
-        plan += [(share_rest, n), *chain[:1], (gate_up, n), (relay_hidden, n - 1)]
-        chain = chain[1:]
+            plan += [(landed, n + 1), (relay, n)]
+        plan += [(share_rest, n), *chain[:1], (relay_hidden, n - 1), (gate_up, n)]
+        chain = chain[1:] if n == 2 else chain
     plan += [(take_second,)] * (remote != 3)
-    plan += [*chain[:1], (relay, remote), *chain[1:]]
-    plan += [(share_rest, remote), (gate_up, remote), (relay_hidden, remote - 1), (heads,)]
+    plan += [(relay, remote), (share_rest, remote), (gate_up, remote)]
     plan += [(wait_loads, weight_loads[2:3])]
-    plan += [(down, 1)] if remote > 1 else []
-    plan += [(project,)]
-    plan += [(origin, 1)] if remote > 1 else []
-    plan += [(relay_hidden, remote), (reduce.start_passed, 0), (reduce.start_finals, 0)]
-    plan += [(finish_dispatch,)]
-    plan += [(down, n) for n in range(2, remote)]
-    plan += [(down, 0), (down, remote)]
-    plan += [(origin, n) for n in [remote, *range(remote - 1, 1, -1)]]
-    plan += [(reduce_pass,), (run,), (finish_hidden,), (reduce_last,), (collect,)]
+    plan += [(down, 1)] if remote > 2 else []
+    plan += [*chain[:1], (relay_hidden, remote - 1)]
+    plan += [(origin, 1)] if remote > 2 else []
+    plan += [*chain[1:], (heads,), (relay_hidden, remote)]
+    for n in range(2 if remote > 2 else 1, remote):
+        plan += [(down, n), (project,), (origin, n)] if n == remote - 1 else [(down, n), (origin, n)]
+    plan += [(reduce.start_passed, 0), (reduce.start_finals, 0), (finish_dispatch,)]
+    plan += [(down, 0), (down, remote), (origin, remote)]
+    plan += [(run, back.parts * (remote - 1)), (reduce_pass,), (run, None)]
+    plan += [(finish_hidden,), (reduce_last,), (collect,)]
     for step, (action, *given) in enumerate(plan):
         with jax.named_scope(f"{action.__name__}#{step}"):
             action(*given)
@@ -1195,7 +1201,7 @@
         dma((chips, 2 * tp_count - 1)),
         dma((2, steps)),
         dma((2, 2, tp_count - 1)),
-        dma((8 * chips,)),
+        dma((14 * chips,)),
     ]
     def kernel(r, k, v, d, a, *refs):
         layer_kernel(tp_count, ep_count, cap, expert_count, (r, k, v, d, a), *refs)

time: 80 us -> 77.5 us (0.969)
  the two profiles are of different devices: /device:TPU:9 before, /device:TPU:0 now
where the time goes in v4:
time: 77.5 us; the launch traced here: 77.3 us
  Pallas kernels  76.5 us (99%)
  between operations  0.8 us (1%)
    pallas_call x1, Pallas kernels, local(): pl.pallas_call(kernel, out_shape=[jax.ShapeDtypeStruct((out_rows, dim), B...  74.6 us
    pallas_call x1, Pallas kernels, settle(): pl.pallas_call(settle_kernel, out_shape=[jax.ShapeDtypeStruct(a.shape, a....  1.95 us

profile of v4, /device:TPU:0, one launch (start us, length us, event | category | flops | bytes accessed | tf_op | source)
XLA Modules:
  0.0 77.3 jit_solution(17291235463860940986)
XLA Ops:
  0.6 74.6 %layer.1 = (bf16[64,4096]{1,0:T(8,128)(2,1)}, bf16[128,1024]{1,0:T(8,128)(2,1)}) custom-call(bf16[256,512]{1,0:T(8,128)(2,1)} %r.1, bf16[256,512]{1,0:T(8,128)(2,1)} %k.1, bf16[256,512]{1,0:T(8,128)(2,1)} %v.1, bf16[256,512]{1,0:T(8,128)(2,1)} %d.1, bf16[256,512]{1,0:T(8,128)(2,1)} %a.1, f32[1,512]{1,0:T(1,128)} %bitcast.11, bf16[512,4096]{1,0:T(8,128)(2,1)} %refs_1_.1, ...), custom_call_target="tpu_custom_call" | custom-call | tf_op jit(solution)/shard_map/layer/pallas_call | solution.py:1209
  75.2 2.0 %settle.1 = (bf16[64,4096]{1,0:T(8,128)(2,1)}, bf16[128,1024]{1,0:T(8,128)(2,1)}) custom-call(bf16[64,4096]{1,0:T(8,128)(2,1)} %get-tuple-element.4.refs_0_, bf16[128,1024]{1,0:T(8,128)(2,1)} %get-tuple-element.5.refs_1_), custom_call_target="tpu_custom_call" | custom-call | tf_op jit(solution)/shard_map/settle/pallas_call | solution.py:1114

commit v5 on v4

--- a/solution.py
+++ b/solution.py
@@ -302,6 +302,15 @@
         self.parts, self.landing = parts, landing
         self.half = parts.shape[2] // 2
         bits = bit_list(count)
+        whole = landing.at[pl.ds(0, count - 1)]
+        self.sent = pltpu.make_async_remote_copy(
+            src_ref=whole,
+            dst_ref=whole,
+            send_sem=sems.at[2 * (count - 1)],
+            recv_sem=sems.at[0],
+            device_id={"tp": flip(self.me, bits[0])},
+            device_id_type=MESH,
+        )
         orders = (bits, bits[::-1])
         self.stages, self.finals, self.copies = [], [], {}
         left = [list(range(count))] * 2
@@ -317,8 +326,8 @@
                     self.copies[stream, delta] = pltpu.make_async_remote_copy(
                         src_ref=parts.at[owner, :, at],
                         dst_ref=landing.at[delta, :, at],
-                        send_sem=sems.at[0, stream, delta - 1],
-                        recv_sem=sems.at[1, stream, delta - 1],
+                        send_sem=sems.at[2 * (count - 1)],
+                        recv_sem=sems.at[stream * (count - 1) + delta - 1],
                         device_id={"tp": flip(self.me, bit)},
                         device_id_type=MESH,
                     )
@@ -354,8 +363,7 @@
             out[:, at] = total.astype(BF16)
 
     def finish(self):
-        for copy in self.copies.values():
-            copy.wait_send()
+        self.sent.wait_send()
 
 
 class Dispatch:
@@ -491,16 +499,16 @@
 
     def across(self, k, place):
         ref = self.rows.at[2 * k + self.core, place]
-        return self.remote(ref, self.pair_sems.at[0, k], self.pair_sems.at[1, k], self.partner)
+        return self.remote(ref, self.pair_sems.at[self.chips], self.pair_sems.at[k], self.partner)
 
     def all_across(self, k, other=False):
         ref = self.rows.at[2 * k + (1 - self.core if other else self.core)]
-        return self.remote(ref, self.pair_sems.at[0, k], self.pair_sems.at[1, k], self.partner)
+        return self.remote(ref, self.pair_sems.at[self.chips], self.pair_sems.at[k], self.partner)
 
     def across_info(self, k, other=False):
         core = 1 - self.core if other else self.core
         ref = self.info.at[2 * k + core]
-        return self.remote(ref, self.pair_info.at[0, k], self.pair_info.at[1, k], self.partner)
+        return self.remote(ref, self.pair_info.at[self.chips], self.pair_info.at[k], self.partner)
 
     def sides(self):
         return (
@@ -553,9 +561,9 @@
             for half in (0, 1):
                 pl.when(moving)(self.along(k, half, way, to).wait_send)
             pl.when(moving)(self.along_info(k, way, to).wait_send)
-        for k in [self.chip] + order:
-            self.all_across(k).wait_send()
-            self.across_info(k).wait_send()
+        for ref, sems in ((self.rows, self.pair_sems), (self.info, self.pair_info)):
+            whole = ref.at[pl.ds(0, self.chips)]
+            self.remote(whole, sems.at[self.chips], sems.at[0], self.partner).wait_send()
 
 
 def chip_order(chip, chips):
@@ -589,8 +597,10 @@
         return pltpu.make_async_remote_copy(
             src_ref=source.at[rows],
             dst_ref=target.at[at, rows],
-            send_sem=self.sems.at[2 * self.chips + self.parts * at + part],
-            recv_sem=self.sems.at[self.chips * (2 + self.parts * kind) + self.parts * at + part],
+            send_sem=self.sems.at[0],
+            recv_sem=self.sems.at[
+                2 + self.chips + self.parts * (self.chips * (kind - 1) + at) + part
+            ],
             device_id={"ep": to},
             device_id_type=MESH,
         )
@@ -599,8 +609,8 @@
         return pltpu.make_async_remote_copy(
             src_ref=self.placed.at[2 * at + 1 - self.core],
             dst_ref=self.pair_in.at[at],
-            send_sem=self.sems.at[at],
-            recv_sem=self.sems.at[self.chips + at],
+            send_sem=self.sems.at[1],
+            recv_sem=self.sems.at[2 + at],
             device_id={"ep": self.partner},
             device_id_type=MESH,
         )
@@ -641,6 +651,7 @@
 
     def relays(self):
         chips, chip, parts = self.chips, self.chip, self.parts
+        order = [1, *range(chips - 1, 1, -1)]
         ready = set()
 
         def summed(at):
@@ -650,7 +661,7 @@
 
         def step(near, number):
             part = number % parts
-            right_at = 1 + number // parts
+            right_at = order[number // parts]
             left_at = chips - 1 - right_at
 
             def rightward():
@@ -666,8 +677,8 @@
         items = parts * (chips - 1)
         for number in range(items + parts):
             if number < items:
-                summed(1 + number // parts)
-                summed(chips - 2 - number // parts)
+                summed(order[number // parts])
+                summed(chips - 1 - order[number // parts])
                 step(True, number)
             if number >= parts:
                 step(False, number - parts)
@@ -696,12 +707,18 @@
                     ).astype(BF16)
 
     def finish(self):
-        for at in range(self.chips):
-            self.pair(at).wait_send()
-            for part in range(self.parts):
-                item = (at, part)
-                pl.when(at > self.chip)(self.right(item).wait_send)
-                pl.when(at < self.chip)(self.left(item).wait_send)
+        for whole, sem in (
+            (self.from_left.at[pl.ds(0, self.chips - 1)], 0),
+            (self.placed.at[pl.ds(0, self.chips)], 1),
+        ):
+            pltpu.make_async_remote_copy(
+                src_ref=whole,
+                dst_ref=whole,
+                send_sem=self.sems.at[sem],
+                recv_sem=self.sems.at[2],
+                device_id={"ep": self.partner},
+                device_id_type=MESH,
+            ).wait_send()
 
 
 def layer_kernel(
@@ -798,7 +815,7 @@
             )
         )
     ]
-    for load in moe_loads + small_loads + mixer_loads + weight_loads:
+    for load in moe_loads:
         load.start()
 
     barrier = pltpu.get_barrier_semaphore()
@@ -811,6 +828,8 @@
     for step in steps:
         pl.when(place + step < ep_count)(lambda: signal("ep", place + step))
         pl.when(place >= step)(lambda: signal("ep", place - step))
+    for load in small_loads + weight_loads[:2] + mixer_loads + weight_loads[2:]:
+        load.start()
     peers = sum(
         jnp.where(place + step < ep_count, 1, 0) + jnp.where(place >= step, 1, 0)
         for step in steps
@@ -1075,12 +1094,12 @@
     plan += [(down, 1)] if remote > 2 else []
     plan += [*chain[:1], (relay_hidden, remote - 1)]
     plan += [(origin, 1)] if remote > 2 else []
-    plan += [*chain[1:], (heads,), (relay_hidden, remote)]
-    for n in range(2 if remote > 2 else 1, remote):
-        plan += [(down, n), (project,), (origin, n)] if n == remote - 1 else [(down, n), (origin, n)]
-    plan += [(reduce.start_passed, 0), (reduce.start_finals, 0), (finish_dispatch,)]
-    plan += [(down, 0), (down, remote), (origin, remote)]
-    plan += [(run, back.parts * (remote - 1)), (reduce_pass,), (run, None)]
+    plan += [*chain[1:], (heads,), (relay_hidden, remote), (project,)]
+    plan += [(reduce.start_passed, 0), (reduce.start_finals, 0)]
+    plan += [(down, n) for n in range(2 if remote > 2 else 1, remote + 1)]
+    plan += [(origin, n) for n in range(remote, 1 if remote > 2 else 0, -1)]
+    plan += [(finish_dispatch,), (down, 0)]
+    plan += [(run, back.parts + 2), (reduce_pass,), (run, None)]
     plan += [(finish_hidden,), (reduce_last,), (collect,)]
     for step, (action, *given) in enumerate(plan):
         with jax.named_scope(f"{action.__name__}#{step}"):
@@ -1194,14 +1213,14 @@
         dma((12,)),
         dma((3, chips, 2)),
         dma((3, chips)),
-        dma((2, chips)),
-        dma((2, chips)),
+        dma((chips + 1,)),
+        dma((chips + 1,)),
         dma((2, 2, 2)),
         dma((chips - 1, 2 * tp_count - 1)),
         dma((chips, 2 * tp_count - 1)),
         dma((2, steps)),
-        dma((2, 2, tp_count - 1)),
-        dma((14 * chips,)),
+        dma((2 * tp_count - 1,)),
+        dma((2 + 9 * chips,)),
     ]
     def kernel(r, k, v, d, a, *refs):
         layer_kernel(tp_count, ep_count, cap, expert_count, (r, k, v, d, a), *refs)

time: 77.5 us -> 74.6 us (0.963)
  the two profiles are of different devices: /device:TPU:0 before, /device:TPU:9 now
where the time goes in v5:
time: 74.6 us; the launch traced here: 74.4 us
  Pallas kernels  73.6 us (99%)
  between operations  0.8 us (1%)
    pallas_call x1, Pallas kernels, local(): pl.pallas_call(kernel, out_shape=[jax.ShapeDtypeStruct((out_rows, dim), B...  71.7 us
    pallas_call x1, Pallas kernels, settle(): pl.pallas_call(settle_kernel, out_shape=[jax.ShapeDtypeStruct(a.shape, a....  1.95 us

profile of v5, /device:TPU:9, one launch (start us, length us, event | category | flops | bytes accessed | tf_op | source)
XLA Modules:
  0.0 74.4 jit_solution(8247406887688118074)
XLA Ops:
  0.6 71.7 %layer.1 = (bf16[64,4096]{1,0:T(8,128)(2,1)}, bf16[128,1024]{1,0:T(8,128)(2,1)}) custom-call(bf16[256,512]{1,0:T(8,128)(2,1)} %r.1, bf16[256,512]{1,0:T(8,128)(2,1)} %k.1, bf16[256,512]{1,0:T(8,128)(2,1)} %v.1, bf16[256,512]{1,0:T(8,128)(2,1)} %d.1, bf16[256,512]{1,0:T(8,128)(2,1)} %a.1, f32[1,512]{1,0:T(1,128)} %bitcast.11, bf16[512,4096]{1,0:T(8,128)(2,1)} %refs_1_.1, ...), custom_call_target="tpu_custom_call" | custom-call | tf_op jit(solution)/shard_map/layer/pallas_call | solution.py:1228
  72.3 2.0 %settle.1 = (bf16[64,4096]{1,0:T(8,128)(2,1)}, bf16[128,1024]{1,0:T(8,128)(2,1)}) custom-call(bf16[64,4096]{1,0:T(8,128)(2,1)} %get-tuple-element.4.refs_0_, bf16[128,1024]{1,0:T(8,128)(2,1)} %get-tuple-element.5.refs_1_), custom_call_target="tpu_custom_call" | custom-call | tf_op jit(solution)/shard_map/settle/pallas_call | solution.py:1133

commit v6 on v5

--- a/solution.py
+++ b/solution.py
@@ -534,12 +534,14 @@
         to = jnp.where(right, self.chip + 1, self.chip - 1)
         return (to >= 0) & (to < self.chips), jnp.where(right, 0, 1), to
 
-    def landed(self, k, exchange):
+    def landed_half(self, k, exchange, half):
         moving, way, to = self.onward(k)
-        for half in (0, 1):
-            self.along(k, half, way, to).wait_recv()
-            pl.when(moving)(self.along(k, half, way, to).start)
-            exchange.start((half,))
+        self.along(k, half, way, to).wait_recv()
+        pl.when(moving)(self.along(k, half, way, to).start)
+        exchange.start((half,))
+
+    def landed_rest(self, k):
+        moving, way, to = self.onward(k)
         self.across(k, self.tp).start()
         self.along_info(k, way, to).wait_recv()
         pl.when(moving)(self.along_info(k, way, to).start)
@@ -935,8 +937,16 @@
             placed[source] = dot_cols(pick.astype(BF16), mine).astype(BF16)
         back.pair(k).start()
 
+    def landed_half(n, half):
+        dispatch.landed_half(sources[n], exchanges[n], half)
+
+    def landed_rest(n):
+        dispatch.landed_rest(sources[n])
+
     def landed(n):
-        dispatch.landed(sources[n], exchanges[n])
+        landed_half(n, 0)
+        landed_half(n, 1)
+        landed_rest(n)
 
     def relay(n):
         exchanges[n].relay()
@@ -1069,9 +1079,10 @@
     more = [(tables, b) for b in range(blocks)]
     chain = [(prefix_step, number) for number in range(len(steps))]
     all_mixer = pltpu.make_async_copy(mix_in, mix_in, load_sems.at[1])
-    plan = [(wait_loads, [all_mixer]), *more[:1], (landed, 1)]
+    plan = [(wait_loads, [all_mixer]), *more[:1], (landed_half, 1, 0)]
+    plan += [(wait_loads, weight_loads[:2]), (gate_up, 0), (landed_half, 1, 1), (landed_rest, 1)]
     plan += [(landed_inner, 2)] * (remote > 1)
-    plan += [(wait_loads, weight_loads[:2]), (gate_up, 0), *more[1:2]]
+    plan += [*more[1:2]]
     plan += [(relay, 1), (dispatch.passing,)] if remote > 1 else []
     plan += [(landed_inner, 3)] * (remote > 2)
     plan += [(landed_outer, 2)] * (remote > 1)

time: 74.6 us -> 74.1 us (level)
  no operation moved by 1% of the time
where the time goes in v6:
time: 74.1 us; the launch traced here: 74 us
  Pallas kernels  73.2 us (99%)
  between operations  0.8 us (1%)
    pallas_call x1, Pallas kernels, local(): pl.pallas_call(kernel, out_shape=[jax.ShapeDtypeStruct((out_rows, dim), B...  71.2 us
    pallas_call x1, Pallas kernels, settle(): pl.pallas_call(settle_kernel, out_shape=[jax.ShapeDtypeStruct(a.shape, a....  1.95 us

profile of v6, /device:TPU:9, one launch (start us, length us, event | category | flops | bytes accessed | tf_op | source)
XLA Modules:
  0.0 74.0 jit_solution(6790660226629339024)
XLA Ops:
  0.6 71.2 %layer.1 = (bf16[64,4096]{1,0:T(8,128)(2,1)}, bf16[128,1024]{1,0:T(8,128)(2,1)}) custom-call(bf16[256,512]{1,0:T(8,128)(2,1)} %r.1, bf16[256,512]{1,0:T(8,128)(2,1)} %k.1, bf16[256,512]{1,0:T(8,128)(2,1)} %v.1, bf16[256,512]{1,0:T(8,128)(2,1)} %d.1, bf16[256,512]{1,0:T(8,128)(2,1)} %a.1, f32[1,512]{1,0:T(1,128)} %bitcast.11, bf16[512,4096]{1,0:T(8,128)(2,1)} %refs_1_.1, ...), custom_call_target="tpu_custom_call" | custom-call | tf_op jit(solution)/shard_map/layer/pallas_call | solution.py:1239
  71.9 2.0 %settle.1 = (bf16[64,4096]{1,0:T(8,128)(2,1)}, bf16[128,1024]{1,0:T(8,128)(2,1)}) custom-call(bf16[64,4096]{1,0:T(8,128)(2,1)} %get-tuple-element.4.refs_0_, bf16[128,1024]{1,0:T(8,128)(2,1)} %get-tuple-element.5.refs_1_), custom_call_target="tpu_custom_call" | custom-call | tf_op jit(solution)/shard_map/settle/pallas_call | solution.py:1144
